TPU v7x, 256 devices: a whole 4x4x8 slice. The times are simulated.
256 devices in a mesh: fs: 32 (over z, x), rep: 4 (over y), tp: 2 (over core).
Axes of the slice: x: 4, y: 4, z: 8, core: 2. Of those that a mesh axis runs over, the one named last changes fastest.
Arguments:
- inputs: bfloat16 [16384, 2048], P(('fs', 'rep')), may hold values from -24 to 24
- query_cot: bfloat16 [16384, 1024], P(('fs', 'rep'), 'tp'), may hold values from -0.046875 to 0.046875
- attended: bfloat16 [16384, 1024], P(('fs', 'rep')), may hold values from -24 to 24
- output_cot: bfloat16 [16384, 2048], P(('fs', 'rep'), 'tp'), may hold values from -0.046875 to 0.046875
- proj_query: bfloat16 [2048, 256], P('fs'), may hold values from -0.125 to 0.125
- proj_output: bfloat16 [1024, 256], P('fs'), may hold values from -0.1875 to 0.1875
- weight_query: float32 [2048, 1024], P('fs', 'tp'), may hold values from -0.125 to 0.125
- weight_output: float32 [1024, 2048], P('fs', 'tp'), may hold values from -0.1875 to 0.1875
- first_query: float32 [256, 1024], P('fs', 'tp'), may hold values from -6 to 6
- second_query: float32 [256, 1024], P('fs', 'tp'), may hold values from 0.0002 to 2
- first_output: float32 [256, 2048], P('fs', 'tp'), may hold values from -6 to 6
- second_output: float32 [256, 2048], P('fs', 'tp'), may hold values from 0.0002 to 2
Outputs:
- new_weight_query: float32 [2048, 1024], P('fs', 'tp')
- new_weight_output: float32 [1024, 2048], P('fs', 'tp')
- step_query: float32 [2048, 1024], P('fs', 'tp')
- step_output: float32 [1024, 2048], P('fs', 'tp')
- new_first_query: float32 [256, 1024], P('fs', 'tp')
- new_second_query: float32 [256, 1024], P('fs', 'tp')
- new_first_output: float32 [256, 2048], P('fs', 'tp')
- new_second_output: float32 [256, 2048], P('fs', 'tp')
- copy_query: bfloat16 [2048, 1024], P(None, 'tp')
- copy_output: bfloat16 [1024, 2048], P(None, 'tp')
All inputs are finite; a program needn't handle non-finite values.
Results may differ from a plain program's by a relative error of at most 0.0031.
Values may be sent and summed in bfloat16 or wider, within the bound.
A program may use at most 64 MiB of HBM per device.

v0:
```python
import jax
import jax.numpy as jnp
from jax import lax
from jax.sharding import PartitionSpec as P

D = 2048
DA = 1024
RANK = 256


beta_first = 0.9
beta_second = 0.95
adam_eps = 1e-08
mean_eps = 1e-06
learn_rate = 0.02


def joined_along(pieces, dim):
    shape = list(pieces.shape[1:])
    shape[dim] *= pieces.shape[0]
    return jnp.moveaxis(pieces, 0, dim).reshape(shape)


def one_gather(arrays, axis, dims):
    vector = jnp.concatenate([a.reshape(-1) for a in arrays])
    lines, at, gathered = (lax.all_gather(vector, axis), 0, [])
    for a, dim in zip(arrays, dims):
        pieces = lines[:, at : at + a.size].reshape(-1, *a.shape)
        gathered.append(joined_along(pieces, dim))
        at += a.size
    return tuple(gathered)


def cut_along(shard, dim, devices):
    before, after = (shard.shape[:dim], shard.shape[dim + 1 :])
    return jnp.moveaxis(shard.reshape(*before, devices, -1, *after), dim, 0)


def sent_and_summed(shard, axis, dim):
    pieces = cut_along(shard, dim, lax.axis_size(axis))
    arrived = lax.all_to_all(pieces, axis, split_axis=0, concat_axis=0, tiled=True)
    return arrived.sum(axis=0)


def side_by_side(arrays, axis, dim, along):
    both = jnp.concatenate(arrays, axis=along)
    result, at, gathered = (sent_and_summed(both, axis, dim), 0, [])
    for a in arrays:
        gathered.append(lax.slice_in_dim(result, at, at + a.shape[along], axis=along))
        at += a.shape[along]
    return tuple(gathered)


def from_everyone(shard, axis):
    copies = jnp.broadcast_to(shard, (lax.axis_size(axis), *shard.shape))
    return lax.all_to_all(copies, axis, split_axis=0, concat_axis=0, tiled=True)


def of_everyone(shard, axis):
    everything = from_everyone(shard, axis)
    return jnp.sum(everything, axis=0)


def in_one(arrays, axis):
    ends = [0]
    for a in arrays:
        ends.append(ends[-1] + a.size)
    so_far = of_everyone(jnp.concatenate([a.ravel() for a in arrays]), axis)
    return tuple((so_far[b:e].reshape(a.shape) for a, b, e in zip(arrays, ends, ends[1:])))


def in_one_piece(arrays, axis, dim, along):
    widths = [a.shape[along] for a in arrays]
    both = jnp.concatenate(arrays, axis=along)
    result = lax.all_gather(both, axis, axis=dim, tiled=True)
    return tuple(jnp.split(result, [sum(widths[:k]) for k in range(1, len(widths))], axis=along))


def contract_rows(left, right):
    return lax.dot_general(
        left,
        right,
        (((0,), (0,)), ((), ())),
        precision=lax.Precision.HIGHEST,
        preferred_element_type=jnp.float32,
    )


def moment_update(low_sum, first, second):
    first_new = beta_first * first + (1.0 - beta_first) * low_sum
    second_new = beta_second * second + (1.0 - beta_second) * low_sum * low_sum
    normed = first_new / (jnp.sqrt(second_new) + adam_eps)
    return (first_new, second_new, normed)


def local(
    inputs,
    query_cot,
    attended,
    output_cot,
    proj_query,
    proj_output,
    weight_query,
    weight_output,
    first_query,
    second_query,
    first_output,
    second_output,
):
    whole_query, whole_output = one_gather((proj_query, proj_output), "fs", (0, 0))
    reduced_query = jnp.dot(inputs, whole_query, preferred_element_type=jnp.float32)
    reduced_output = jnp.dot(attended, whole_output, preferred_element_type=jnp.float32)
    part_query = contract_rows(reduced_query, query_cot.astype(jnp.float32))
    part_output = contract_rows(reduced_output, output_cot.astype(jnp.float32))
    low_query, low_output = side_by_side((part_query, part_output), "fs", 0, 1)
    low_query, low_output = in_one((low_query, low_output), "rep")
    first_q, second_q, normed_q = moment_update(low_query, first_query, second_query)
    first_o, second_o, normed_o = moment_update(low_output, first_output, second_output)
    local_total = jnp.sum(normed_q * normed_q) + jnp.sum(normed_o * normed_o)
    total = of_everyone(local_total, ("fs", "tp"))
    scale = lax.rsqrt(total / (RANK * (DA + D)) + mean_eps)
    half_q = normed_q.astype(jnp.bfloat16)
    half_o = normed_o.astype(jnp.bfloat16)
    pieces = in_one_piece((half_q, half_o), "fs", 0, 1)
    update_query = jnp.dot(proj_query, pieces[0], preferred_element_type=jnp.float32)
    update_output = jnp.dot(proj_output, pieces[1], preferred_element_type=jnp.float32)
    step_q = scale * update_query
    step_o = scale * update_output
    new_q = weight_query - learn_rate * step_q
    new_o = weight_output - learn_rate * step_o
    copy_q, copy_o = one_gather(
        (new_q.astype(jnp.bfloat16), new_o.astype(jnp.bfloat16)), "fs", (0, 0)
    )
    return (new_q, new_o, step_q, step_o, first_q, second_q, first_o, second_o, copy_q, copy_o)


def solution(mesh):
    return jax.shard_map(
        local,
        mesh=mesh,
        in_specs=(
            P(("fs", "rep"), None),
            P(("fs", "rep"), "tp"),
            P(("fs", "rep"), None),
            P(("fs", "rep"), "tp"),
            P("fs", None),
            P("fs", None),
            P("fs", "tp"),
            P("fs", "tp"),
            P("fs", "tp"),
            P("fs", "tp"),
            P("fs", "tp"),
            P("fs", "tp"),
        ),
        out_specs=(
            P("fs", "tp"),
            P("fs", "tp"),
            P("fs", "tp"),
            P("fs", "tp"),
            P("fs", "tp"),
            P("fs", "tp"),
            P("fs", "tp"),
            P("fs", "tp"),
            P(None, "tp"),
            P(None, "tp"),
        ),
        check_vma=False,
    )
```

profile of v0, /device:TPU:1, one launch (start us, length us, event | category | flops | bytes accessed | tf_op | source)
XLA Modules:
  0.0 311.5 jit_solution(3104404758752084554)
XLA Ops:
  7.2 0.8 copy.29
  8.0 0.8 copy.28
  8.8 0.6 pad_maximum_fusion.1
  9.5 77.9 %all-gather.5.cloned.1.call-done = bf16[786432]{0:T(1024)(128)(2,1)} async-done(((bf16[24576]{0:T(1024)(128)(2,1)}), bf16[786432]{0:T(1024)(128)(2,1)}) %all-gather.5.cloned.1.call-update) | async-done | bytes 1572880 | tf_op jit(solution)/shard_map/all_gather | solution.py:26
  87.4 1.8 reshape.72
  89.2 0.8 slice.55
  90.7 1.3 reshape_reshape.13
  93.2 0.6 fusion.14
  93.9 39.3 %all_to_all.17 = f32[32,8,1536]{2,1,0:T(8,128)S(1)} all-to-all(f32[32,8,1536]{2,1,0:T(8,128)S(1)} %maximum_bitcast_fusion), channel_id=1, replica_groups=mesh['fs'=32,'rep'=4,'tp'=2] {'fs'}, dimensions={0} | all-to-all | bytes 3145728 | tf_op jit(solution)/shard_map/all_to_all | solution.py:41
  133.5 9.0 %all_to_all.18 = f32[4,1,12288]{2,1,0:T(1,128)S(1)} all-to-all(f32[4,1,12288]{2,1,0:T(1,128)S(1)} %broadcast_in_dim.6), channel_id=1, replica_groups=mesh['fs'=32,'rep'=4,'tp'=2] {'rep'}, dimensions={0} | all-to-all | bytes 393216 | tf_op jit(solution)/shard_map/all_to_all | solution.py:56
  142.8 0.6 multiply_reduce_fusion.1
  143.4 0.6 multiply_reduce_fusion
  145.3 0.6 broadcast_in_dim.7
  146.0 13.5 %all-to-all-start.2 = ((f32[64,1,1]{2,1,0:T(1,128)}), f32[64,1,1]{2,1,0:T(1,128)S(1)}, u32[]{:S(2)}, u32[]{:S(2)}) async-start(f32[64,1,1]{2,1,0:T(1,128)} %broadcast_in_dim.7), calls=%async_computation.2 | async-start | bytes 65536 | tf_op jit(solution)/shard_map/all_to_all | solution.py:56
  159.6 39.1 %all_gather.17 = bf16[256,1536]{1,0:T(8,128)(2,1)S(1)} all-gather(bf16[8,1536]{1,0:T(8,128)(2,1)S(1)} %pad_maximum_fusion.3), channel_id=1, replica_groups=mesh['fs'=32,'rep'=4,'tp'=2] {'fs'}, dimensions={0}, use_global_device_ids=true | all-gather | bytes 811008 | tf_op jit(solution)/shard_map/all_gather | solution.py:75
  198.7 0.7 reduce_sum.49
  200.5 0.7 convert_bitcast_fusion.1
  201.2 0.7 convert_bitcast_fusion
  201.9 0.7 pad_maximum_fusion
  202.6 86.1 %all-gather.7.cloned.1.call-done = bf16[2097152]{0:T(1024)(128)(2,1)} async-done(((bf16[65536]{0:T(1024)(128)(2,1)}), bf16[2097152]{0:T(1024)(128)(2,1)}) %all-gather.7.cloned.1.call-update) | async-done | bytes 4194320 | tf_op jit(solution)/shard_map/all_gather | solution.py:26
  288.7 5.6 %reshape.73 = bf16[32,65536]{1,0:T(8,128)(2,1)} reshape(bf16[2097152]{0:T(1024)(128)(2,1)} %all-gather.7.cloned.1.call-done) | data formatting | bytes 8388608 | tf_op jit(solution)/shard_map/all_gather | solution.py:26
  294.3 3.8 %fusion.10 = (bf16[32,32768]{1,0:T(8,128)(2,1)}, bf16[32,32768]{1,0:T(8,128)(2,1)S(1)}) fusion(bf16[32,65536]{1,0:T(8,128)(2,1)} %reshape.73), kind=kLoop, calls=%fused_computation.30 | loop fusion | bytes 8388608 | tf_op jit(solution)/shard_map/slice | solution.py:28
  298.1 4.2 %reshape_reshape.15 = bf16[1024,1024]{1,0:T(8,128)(2,1)} reshape(bf16[32,32768]{1,0:T(8,128)(2,1)} %get-tuple-element.20) | data formatting | bytes 4194304 | tf_op jit(solution)/shard_map/reshape;reshape | solution.py:21
  302.3 2.3 reshape_reshape.14
  (66 shorter events, 3.0 us)
Async XLA Ops:
  7.2 84.8 %copy-start = (bf16[128,2048]{1,0:T(8,128)(2,1)S(1)}, bf16[128,2048]{1,0:T(8,128)(2,1)}, u32[]{:S(2)}) copy-start(bf16[128,2048]{1,0:T(8,128)(2,1)} %param.12) | copy-start | bytes 1572868
  7.2 80.2 %all-gather.5.cloned.1.call-start = ((), (), s32[]{:S(2)}) async-start(), calls=%async_computation.3 | async-start | bytes 1622016 | tf_op jit(solution)/shard_map/all_gather | solution.py:26
  90.1 2.4 copy-start.3
  90.6 2.2 copy-start.9
  90.7 2.6 copy-start.4
  133.2 9.5 %copy-start.16 = (f32[8,512]{1,0:T(8,128)S(1)}, f32[8,512]{1,0:T(8,128)}, u32[]{:S(2)}) copy-start(f32[8,512]{1,0:T(8,128)} %param.21) | copy-start | bytes 49156
  133.2 9.6 %copy-start.17 = (f32[8,512]{1,0:T(8,128)S(1)}, f32[8,512]{1,0:T(8,128)}, u32[]{:S(2)}) copy-start(f32[8,512]{1,0:T(8,128)} %param.20) | copy-start | bytes 49156
  133.2 10.2 %copy-start.14 = (f32[8,1024]{1,0:T(8,128)S(1)}, f32[8,1024]{1,0:T(8,128)}, u32[]{:S(2)}) copy-start(f32[8,1024]{1,0:T(8,128)} %param.23) | copy-start | bytes 98308
  133.2 10.2 %copy-start.15 = (f32[8,1024]{1,0:T(8,128)S(1)}, f32[8,1024]{1,0:T(8,128)}, u32[]{:S(2)}) copy-start(f32[8,1024]{1,0:T(8,128)} %param.22) | copy-start | bytes 98308
  133.2 66.9 %copy-start.11 = (bf16[32,256]{1,0:T(8,128)(2,1)S(1)}, bf16[32,256]{1,0:T(8,128)(2,1)}, u32[]{:S(2)}) copy-start(bf16[32,256]{1,0:T(8,128)(2,1)} %param.17) | copy-start | bytes 49156
  133.3 67.0 %copy-start.10 = (bf16[64,256]{1,0:T(8,128)(2,1)S(1)}, bf16[64,256]{1,0:T(8,128)(2,1)}, u32[]{:S(2)}) copy-start(bf16[64,256]{1,0:T(8,128)(2,1)} %param.16) | copy-start | bytes 98308
  133.3 67.1 %copy-start.5 = (f32[64,512]{1,0:T(8,128)S(1)}, f32[64,512]{1,0:T(8,128)}, u32[]{:S(2)}) copy-start(f32[64,512]{1,0:T(8,128)} %param.18) | copy-start | bytes 393220
  133.4 67.8 %copy-start.6 = (f32[32,1024]{1,0:T(8,128)S(1)}, f32[32,1024]{1,0:T(8,128)}, u32[]{:S(2)}) copy-start(f32[32,1024]{1,0:T(8,128)} %param.19) | copy-start | bytes 393220
  143.4 150.9 %copy-start.12 = (f32[8,512]{1,0:T(8,128)}, f32[8,512]{1,0:T(8,128)S(1)}, u32[]{:S(2)}) copy-start(f32[8,512]{1,0:T(8,128)S(1)} %get-tuple-element.18) | copy-start | bytes 49156
  143.4 150.9 %copy-start.13 = (f32[8,512]{1,0:T(8,128)}, f32[8,512]{1,0:T(8,128)S(1)}, u32[]{:S(2)}) copy-start(f32[8,512]{1,0:T(8,128)S(1)} %get-tuple-element.19) | copy-start | bytes 49156
  144.0 150.2 %copy-start.7 = (f32[8,1024]{1,0:T(8,128)}, f32[8,1024]{1,0:T(8,128)S(1)}, u32[]{:S(2)}) copy-start(f32[8,1024]{1,0:T(8,128)S(1)} %get-tuple-element.15) | copy-start | bytes 98308
  144.0 150.3 %copy-start.8 = (f32[8,1024]{1,0:T(8,128)}, f32[8,1024]{1,0:T(8,128)S(1)}, u32[]{:S(2)}) copy-start(f32[8,1024]{1,0:T(8,128)S(1)} %get-tuple-element.16) | copy-start | bytes 98308
  146.0 52.7 %all-to-all-start.2 = ((f32[64,1,1]{2,1,0:T(1,128)}), f32[64,1,1]{2,1,0:T(1,128)S(1)}, u32[]{:S(2)}, u32[]{:S(2)}) async-start(f32[64,1,1]{2,1,0:T(1,128)} %broadcast_in_dim.7), calls=%async_computation.2 | async-start | bytes 65536 | tf_op jit(solution)/shard_map/all_to_all | solution.py:56
  159.5 129.2 %all-gather.7.cloned.1.call-start = ((), (), s32[]{:S(2)}) async-start(), calls=%async_computation.4 | async-start | bytes 4325376 | tf_op jit(solution)/shard_map/all_gather | solution.py:26
  200.3 94.0 %copy-start.1 = (f32[32,1024]{1,0:T(8,128)}, f32[32,1024]{1,0:T(8,128)S(1)}, u32[]{:S(2)}) copy-start(f32[32,1024]{1,0:T(8,128)S(1)} %fusion) | copy-start | bytes 393220
  200.5 93.8 %copy-start.2 = (f32[64,512]{1,0:T(8,128)}, f32[64,512]{1,0:T(8,128)S(1)}, u32[]{:S(2)}) copy-start(f32[64,512]{1,0:T(8,128)S(1)} %fusion.1) | copy-start | bytes 393220
Sparse Core Ops, SparseCore 0:
  11.2 76.1 all-gather.4
  202.7 85.9 all-gather.6
where the time goes:
time: 315 us; the launch traced here: 311 us
  waiting for transfers between devices  164 us (52%)
  blocking collectives  87.3 us (28%)
  local copies, waits for them, and re-layouts  23 us (7%)
  between operations  16.4 us (5%)
  starting transfers between devices  13.6 us (4%)
  other arithmetic  5.03 us (2%)
    all_gather x2, waiting for transfers between devices, one_gather(): lines, at, gathered = (lax.all_gather(vector, axis), 0, [])  164 us
    all_to_all x1, blocking collectives, sent_and_summed(): lax.all_to_all(pieces, axis, split_axis=0, concat_axis=0, tiled=True)  39.3 us
    all_gather x1, blocking collectives, in_one_piece(): result = lax.all_gather(both, axis, axis=dim, tiled=True)  39.1 us
    all_to_all x1, starting transfers between devices, from_everyone(): return lax.all_to_all(copies, axis, split_axis=0, concat_axis=0, tiled=True)  13.5 us
    all_to_all x1, blocking collectives, from_everyone(): return lax.all_to_all(copies, axis, split_axis=0, concat_axis=0, tiled=True)  8.98 us
    another operation x4, local copies, waits for them, and re-layouts, joined_along(): return jnp.moveaxis(pieces, 0, dim).reshape(shape)  8.37 us
    all_gather x2, local copies, waits for them, and re-layouts, one_gather(): lines, at, gathered = (lax.all_gather(vector, axis), 0, [])  7.42 us
  transfers between devices with their start and end apart: 3, of which 2 were waited for; matrix products, arithmetic and copies ran while one was open for 0% of the time, Pallas kernels for 0%

commit v1 on v0

v1 whole, which is shorter than its diff:
```python
import functools

import jax
import jax.numpy as jnp
from jax import lax
from jax.experimental import pallas as pl
from jax.experimental.pallas import tpu as pltpu
from jax.sharding import PartitionSpec as P

D = 2048
DA = 1024
RANK = 256
NZ, NX, NY = 8, 4, 4

beta_first = 0.9
beta_second = 0.95
adam_eps = 1e-08
mean_eps = 1e-06
learn_rate = 0.02
HALF = 768

MESH = pl.DeviceIdType.MESH
NEAR_FIRST = (1, 7, 2, 6, 3, 5, 4)


def moment_update(low_sum, first, second):
    first_new = beta_first * first + (1.0 - beta_first) * low_sum
    second_new = beta_second * second + (1.0 - beta_second) * low_sum * low_sum
    normed = first_new / (jnp.sqrt(second_new) + adam_eps)
    return (first_new, second_new, normed)


def coded(v):
    square = v * v
    fourth = square * square
    return jnp.where(v < 0, -fourth, fourth).astype(jnp.bfloat16)


def decoded(c):
    c = c.astype(jnp.float32)
    root = lax.rsqrt(lax.rsqrt(jnp.maximum(jnp.abs(c), 1e-37)))
    return jnp.where(c < 0, -root, root)


def comm_kernel(
    inputs, query_cot, attended, output_cot, proj_q, proj_o, w_q, w_o,
    first_q, second_q, first_o, second_o,
    pq, po, half, low, scale, wg_q, wg_o,
    x_in, c_q, x_at, c_o, fst, snd, old_q, old_o, code_q, code_o,
    lb, cb, by, bx, sz, bz, ty, by2, qc, qz, qx, qy,
    loc, a_zs, a_zr, a_xs, a_xr, a_cs, a_cr,
    w_xs, w_xr, w_zs, w_zr, w_ys, w_yr,
    b_ys, b_yr, b_xs, b_xr, b_zs, b_zr, b_2s, b_2r, b_ls, b_lr,
    e_zs, e_zr, e_xs, e_xr, e_ys, e_yr,
    q_cs, q_cr, q_zs, q_zr, q_xs, q_xr, q_ys, q_yr,
):
    f = lax.axis_index("fs")
    y = lax.axis_index("rep")
    t = lax.axis_index("tp")
    z = f // NX
    x = f % NX
    p = y % 2
    o = 1 - p

    def at_z(d):
        return {"fs": ((z + d) % NZ) * NX + x}

    def at_x(e):
        return {"fs": z * NX + (x + e) % NX}

    def at_y(s):
        return {"rep": (y + s) % NY}

    other_core = {"tp": 1 - t}
    sends = []

    def remote(src, dst, ssem, rsem, dev):
        return pltpu.make_async_remote_copy(
            src_ref=src, dst_ref=dst, send_sem=ssem, recv_sem=rsem,
            device_id=dev, device_id_type=MESH,
        )

    def send(src, dst, ssem, rsem, dev):
        c = remote(src, dst, ssem, rsem, dev)
        c.start()
        sends.append(c)

    def arrived(dst, rsem):
        remote(dst, dst, rsem, rsem, other_core).wait_recv()

    loads = [
        pltpu.make_async_copy(proj_q.at[t], pq.at[f, t], loc.at[0]),
        pltpu.make_async_copy(proj_o.at[t], po.at[f, t], loc.at[1]),
        pltpu.make_async_copy(inputs, x_in, loc.at[2]),
        pltpu.make_async_copy(attended, x_at, loc.at[3]),
        pltpu.make_async_copy(query_cot, c_q, loc.at[4]),
        pltpu.make_async_copy(output_cot, c_o, loc.at[5]),
        pltpu.make_async_copy(first_q, fst.at[0, :, pl.ds(0, 512)], loc.at[6]),
        pltpu.make_async_copy(first_o.at[:, pl.ds(0, 256)], fst.at[0, :, pl.ds(512, 256)], loc.at[7]),
        pltpu.make_async_copy(first_o.at[:, pl.ds(256, 768)], fst.at[1], loc.at[8]),
        pltpu.make_async_copy(second_q, snd.at[0, :, pl.ds(0, 512)], loc.at[9]),
        pltpu.make_async_copy(second_o.at[:, pl.ds(0, 256)], snd.at[0, :, pl.ds(512, 256)], loc.at[10]),
        pltpu.make_async_copy(second_o.at[:, pl.ds(256, 768)], snd.at[1], loc.at[11]),
        pltpu.make_async_copy(w_q.at[p], old_q, loc.at[12]),
        pltpu.make_async_copy(w_o.at[p], old_o, loc.at[13]),
    ]
    for c in loads:
        c.start()

    barrier = pltpu.get_barrier_semaphore()
    peers = [at_z(d) for d in range(1, NZ)] + [at_x(e) for e in range(1, NX)]
    peers += [at_y(s) for s in range(1, NY)] + [other_core]
    for dev in peers:
        pl.semaphore_signal(barrier, inc=1, device_id=dev, device_id_type=MESH)
    pl.semaphore_wait(barrier, len(peers))

    loads[0].wait()
    loads[1].wait()
    for d in NEAR_FIRST:
        send(pq.at[f, t], pq.at[f, t], a_zs.at[0, d], a_zr.at[0, d], at_z(d))
        send(po.at[f, t], po.at[f, t], a_zs.at[1, d], a_zr.at[1, d], at_z(d))
    for d in (0,) + NEAR_FIRST:
        g = ((z + NZ - d) % NZ) * NX + x
        if d:
            arrived(pq.at[g, t], a_zr.at[0, d])
            arrived(po.at[g, t], a_zr.at[1, d])
        for e in range(1, NX):
            send(pq.at[g, t], pq.at[g, t], a_xs.at[0, d, e], a_xr.at[0, d, e], at_x(e))
            send(po.at[g, t], po.at[g, t], a_xs.at[1, d, e], a_xr.at[1, d, e], at_x(e))

    for c in loads[12:14]:
        c.wait()
    code_q[...] = coded(old_q[...])
    code_o[...] = coded(old_o[...])
    out_q = pltpu.make_async_copy(code_q, wg_q.at[f, p], loc.at[12])
    out_o = pltpu.make_async_copy(code_o, wg_o.at[f, p], loc.at[13])
    out_q.start()
    out_o.start()
    for e in range(1, NX):
        send(code_q, wg_q.at[f, p], w_xs.at[0, e], w_xr.at[0, e], at_x(e))
        send(code_o, wg_o.at[f, p], w_xs.at[1, e], w_xr.at[1, e], at_x(e))

    for d in (0,) + NEAR_FIRST:
        row = ((z + NZ - d) % NZ) * NX
        for e in range(1, NX):
            g = row + (x + NX - e) % NX
            arrived(pq.at[g, t], a_xr.at[0, d, e])
            arrived(po.at[g, t], a_xr.at[1, d, e])
        for k, ref in enumerate((pq, po)):
            part = ref.at[pl.ds(row, NX), t]
            send(part, part, a_cs.at[k, d], a_cr.at[k, d], other_core)
    for d in (0,) + NEAR_FIRST:
        row = ((z + NZ - d) % NZ) * NX
        for k, ref in enumerate((pq, po)):
            arrived(ref.at[pl.ds(row, NX), 1 - t], a_cr.at[k, d])

    for c in loads[2:6]:
        c.wait()

    def partial_low(tokens, whole, cot, depth):
        reduced = jnp.dot(
            tokens[...], whole[...].reshape(depth, RANK), preferred_element_type=jnp.float32
        )
        high = reduced.astype(jnp.bfloat16)
        rest = (reduced - high.astype(jnp.float32)).astype(jnp.bfloat16)
        both = jnp.concatenate([high, rest], axis=0)
        return lax.dot_general(
            both, jnp.concatenate([cot, cot], axis=0),
            (((0,), (0,)), ((), ())), preferred_element_type=jnp.float32,
        )

    def put(par, lo, block):
        for zz in range(NZ):
            for xx in range(NX):
                r = (zz * NX + xx) * 8
                lb[par, xx, zz, :, lo : lo + block.shape[1]] = block[r : r + 8, :]

    low_o = partial_low(x_at, po, c_o[...], DA)
    put(0, 512, low_o[:, :256])
    put(1, 0, low_o[:, 256:])
    put(0, 0, partial_low(x_in, pq, c_q[...], D))

    for j in range(NX):
        cb[j] = coded(lb[o, j])
        send(cb.at[j], by.at[j], b_ys.at[j], b_yr.at[j], at_y(1 if j < 2 else -1 + NY))

    def weights(s):
        if s == 0:
            out_q.wait()
            out_o.wait()
            for e in range(1, NX):
                g = z * NX + (x + NX - e) % NX
                arrived(wg_q.at[g, p], w_xr.at[0, e])
                arrived(wg_o.at[g, p], w_xr.at[1, e])
        groups = []
        for way, sign in ((0, 1), (1, -1)):
            row = ((z - sign * s + NZ) % NZ) * NX
            for k, ref in enumerate((wg_q, wg_o)):
                if s == 4 and way != k:
                    continue
                part = ref.at[pl.ds(row, NX), p]
                if s:
                    arrived(part, w_zr.at[way, k, s])
                if s < 3 or (s == 3 and way == k):
                    send(part, part, w_zs.at[way, k, s + 1], w_zr.at[way, k, s + 1], at_z(sign % NZ))
                if s or way == 0:
                    groups.append((way, k, ref, row))
        for way, k, ref, row in groups:
            for side in range(2):
                two = ref.at[pl.ds(row + 2 * side, 2), p]
                send(two, two, w_ys.at[way, k, s, side], w_yr.at[way, k, s, side],
                     at_y(1 if side == 0 else NY - 1))

    def weights_y(s):
        for way, sign in ((0, 1), (1, -1)):
            row = ((z - sign * s + NZ) % NZ) * NX
            for k, ref in enumerate((wg_q, wg_o)):
                if (s == 4 and way != k) or (s == 0 and way):
                    continue
                for side in range(2):
                    arrived(ref.at[pl.ds(row + 2 * side, 2), o], w_yr.at[way, k, s, side])

    weights(0)

    for e in (1, 2, 3, 0):
        j = (x + e) % NX
        arrived(by.at[j], b_yr.at[j])
        lb[p, j] = lb[p, j] + decoded(by[j])
        if e:
            cb[NX + e - 1] = coded(lb[p, j])
            send(cb.at[NX + e - 1], bx.at[e - 1], b_xs.at[e - 1], b_xr.at[e - 1], at_x(e))
    weights(1)
    for e in range(3):
        arrived(bx.at[e], b_xr.at[e])
    mine = (lb[p, x] + decoded(bx[0])) + (decoded(bx[1]) + decoded(bx[2]))
    lb[o, 0] = mine
    sz[...] = coded(mine)
    for d in NEAR_FIRST:
        send(sz.at[(z + d) % NZ], bz.at[d - 1], b_zs.at[d - 1], b_zr.at[d - 1], at_z(d))
    weights(2)
    for d in NEAR_FIRST:
        arrived(bz.at[d - 1], b_zr.at[d - 1])
    mine = lb[o, 0, z]
    for d in range(7):
        mine = mine + decoded(bz[d])
    ty[...] = mine
    send(ty, by2, b_2s.at[0], b_2r.at[0], at_y(2))
    for c in loads[6:12]:
        c.wait()
    arrived(by2, b_2r.at[0])

    low_sum = mine + by2[...]
    low[p] = low_sum
    _, _, normed = moment_update(low_sum, fst[p], snd[p])
    half[f, :, pl.ds(pl.multiple_of(p * HALF, 256), HALF)] = normed.astype(jnp.bfloat16)
    square = normed * normed
    total = square[:, 0:128]
    for k in range(1, 6):
        total = total + square[:, k * 128 : (k + 1) * 128]
    qc[0] = total

    def piece(g, n, par):
        return half.at[pl.ds(g, n), :, pl.ds(pl.multiple_of(par * HALF, 256), HALF)]

    send(qc.at[0], qc.at[1], q_cs.at[0], q_cr.at[0], other_core)
    for d in NEAR_FIRST:
        send(piece(f, 1, p), piece(f, 1, p), e_zs.at[d], e_zr.at[d], at_z(d))
    send(low.at[p], low.at[p], b_ls.at[0], b_lr.at[0], at_y(1))
    arrived(qc.at[1], q_cr.at[0])
    qz[z] = total + qc[1]
    for d in NEAR_FIRST:
        send(qz.at[z], qz.at[z], q_zs.at[d], q_zr.at[d], at_z(d))
    for d in (0,) + NEAR_FIRST:
        g = ((z + NZ - d) % NZ) * NX + x
        if d:
            arrived(piece(g, 1, p), e_zr.at[d])
        for e in range(1, NX):
            send(piece(g, 1, p), piece(g, 1, p), e_xs.at[d, e], e_xr.at[d, e], at_x(e))
    for d in NEAR_FIRST:
        arrived(qz.at[(z + NZ - d) % NZ], q_zr.at[d])
    total = qz[0]
    for k in range(1, NZ):
        total = total + qz[k]
    qx[x] = total
    for e in range(1, NX):
        send(qx.at[x], qx.at[x], q_xs.at[e], q_xr.at[e], at_x(e))
    for d in (0,) + NEAR_FIRST:
        row = ((z + NZ - d) % NZ) * NX
        for e in range(1, NX):
            arrived(piece(row + (x + NX - e) % NX, 1, p), e_xr.at[d, e])
        for side in range(2):
            two = piece(row + 2 * side, 2, p)
            send(two, two, e_ys.at[d, side], e_yr.at[d, side], at_y(1 if side == 0 else NY - 1))
    for e in range(1, NX):
        arrived(qx.at[(x + NX - e) % NX], q_xr.at[e])
    qy[p] = (qx[0] + qx[1]) + (qx[2] + qx[3])
    send(qy.at[p], qy.at[p], q_ys.at[0], q_yr.at[0], at_y(1))
    weights(3)
    arrived(low.at[o], b_lr.at[0])
    arrived(qy.at[o], q_yr.at[0])
    total = jnp.sum(qy[0] + qy[1])
    scale[...] = lax.rsqrt(jnp.full((8, 128), total) / (RANK * (DA + D)) + mean_eps)
    for d in (0,) + NEAR_FIRST:
        row = ((z + NZ - d) % NZ) * NX
        for side in range(2):
            arrived(piece(row + 2 * side, 2, o), e_yr.at[d, side])
    weights(4)
    for s in range(5):
        weights_y(s)
    for c in sends:
        c.wait_send()


def gathered(inputs, query_cot, attended, output_cot, proj_q, proj_o, w_q, w_o,
             first_q, second_q, first_o, second_o):
    f32, bf16 = jnp.float32, jnp.bfloat16
    vmem = pl.BlockSpec(memory_space=pltpu.VMEM)
    anywhere = pl.BlockSpec(memory_space=pl.ANY)
    dma = pltpu.SemaphoreType.DMA
    return pl.pallas_call(
        comm_kernel,
        out_shape=(
            jax.ShapeDtypeStruct((32, 2, 32, RANK), bf16),
            jax.ShapeDtypeStruct((32, 2, 16, RANK), bf16),
            jax.ShapeDtypeStruct((32, 8, 2 * HALF), bf16),
            jax.ShapeDtypeStruct((2, 8, HALF), f32),
            jax.ShapeDtypeStruct((8, 128), f32),
            jax.ShapeDtypeStruct((32, 2, 32, 512), bf16),
            jax.ShapeDtypeStruct((32, 2, 16, 1024), bf16),
        ),
        in_specs=[anywhere] * 12,
        out_specs=(vmem, vmem, vmem, vmem, vmem, anywhere, anywhere),
        scratch_shapes=[
            pltpu.VMEM((128, D), bf16),
            pltpu.VMEM((128, 512), bf16),
            pltpu.VMEM((128, DA), bf16),
            pltpu.VMEM((128, 1024), bf16),
            pltpu.VMEM((2, 8, HALF), f32),
            pltpu.VMEM((2, 8, HALF), f32),
            pltpu.VMEM((32, 512), f32),
            pltpu.VMEM((16, 1024), f32),
            pltpu.VMEM((32, 512), bf16),
            pltpu.VMEM((16, 1024), bf16),
            pltpu.VMEM((2, NX, NZ, 8, HALF), f32),
            pltpu.VMEM((7, NZ, 8, HALF), bf16),
            pltpu.VMEM((NX, NZ, 8, HALF), bf16),
            pltpu.VMEM((3, NZ, 8, HALF), bf16),
            pltpu.VMEM((NZ, 8, HALF), bf16),
            pltpu.VMEM((7, 8, HALF), bf16),
            pltpu.VMEM((8, HALF), f32),
            pltpu.VMEM((8, HALF), f32),
            pltpu.VMEM((2, 8, 128), f32),
            pltpu.VMEM((NZ, 8, 128), f32),
            pltpu.VMEM((NX, 8, 128), f32),
            pltpu.VMEM((2, 8, 128), f32),
            dma((14,)),
            dma((2, 8)), dma((2, 8)), dma((2, 8, 4)), dma((2, 8, 4)), dma((2, 8)), dma((2, 8)),
            dma((2, 4)), dma((2, 4)), dma((2, 2, 5)), dma((2, 2, 5)), dma((2, 2, 5, 2)), dma((2, 2, 5, 2)),
            dma((4,)), dma((4,)), dma((3,)), dma((3,)), dma((7,)), dma((7,)),
            dma((1,)), dma((1,)), dma((1,)), dma((1,)),
            dma((8,)), dma((8,)), dma((8, 4)), dma((8, 4)), dma((8, 2)), dma((8, 2)),
            dma((1,)), dma((1,)), dma((8,)), dma((8,)), dma((4,)), dma((4,)), dma((1,)), dma((1,)),
        ],
        compiler_params=pltpu.CompilerParams(collective_id=0, has_side_effects=True),
    )(
        inputs, query_cot, attended, output_cot,
        proj_q.reshape(2, 32, RANK), proj_o.reshape(2, 16, RANK),
        w_q, w_o, first_q, second_q, first_o, second_o,
    )


def local(
    inputs, query_cot, attended, output_cot, proj_query, proj_output,
    weight_query, weight_output, first_query, second_query, first_output, second_output,
):
    pq, po, half, low, scale_tile, wg_q, wg_o = gathered(
        inputs, query_cot, attended, output_cot, proj_query, proj_output,
        weight_query.reshape(2, 32, 512), weight_output.reshape(2, 16, 1024),
        first_query, second_query, first_output, second_output,
    )
    whole_q, whole_o = pq.reshape(D, RANK), po.reshape(DA, RANK)
    half = half.reshape(RANK, 2 * HALF)
    half_q, half_o = half[:, :512], half[:, 512:]
    scale = scale_tile[0, 0]
    low_q = low[0, :, :512]
    low_o = jnp.concatenate([low[0, :, 512:], low[1]], axis=1)
    first_q, second_q, _ = moment_update(low_q, first_query, second_query)
    first_o, second_o, _ = moment_update(low_o, first_output, second_output)
    step_q = scale * jnp.dot(proj_query, half_q, preferred_element_type=jnp.float32)
    step_o = scale * jnp.dot(proj_output, half_o, preferred_element_type=jnp.float32)
    new_q = weight_query - learn_rate * step_q
    new_o = weight_output - learn_rate * step_o
    all_q = scale * jnp.dot(whole_q, half_q, preferred_element_type=jnp.float32)
    all_o = scale * jnp.dot(whole_o, half_o, preferred_element_type=jnp.float32)
    old_q = decoded(wg_q.reshape(D, 512))
    old_o = decoded(wg_o.reshape(DA, 1024))
    copy_q = (old_q - learn_rate * all_q).astype(jnp.bfloat16)
    copy_o = (old_o - learn_rate * all_o).astype(jnp.bfloat16)
    return (new_q, new_o, step_q, step_o, first_q, second_q, first_o, second_o, copy_q, copy_o)


def solution(mesh):
    return jax.shard_map(
        local,
        mesh=mesh,
        in_specs=(
            P(("fs", "rep"), None),
            P(("fs", "rep"), "tp"),
            P(("fs", "rep"), None),
            P(("fs", "rep"), "tp"),
            P("fs", None),
            P("fs", None),
            P("fs", "tp"),
            P("fs", "tp"),
            P("fs", "tp"),
            P("fs", "tp"),
            P("fs", "tp"),
            P("fs", "tp"),
        ),
        out_specs=(
            P("fs", "tp"),
            P("fs", "tp"),
            P("fs", "tp"),
            P("fs", "tp"),
            P("fs", "tp"),
            P("fs", "tp"),
            P("fs", "tp"),
            P("fs", "tp"),
            P(None, "tp"),
            P(None, "tp"),
        ),
        check_vma=False,
    )
```

time: 315 us -> 94.7 us (0.30); the launches traced: 311 us -> 94.4 us
  waiting for transfers between devices: 164 us -> 0 us
  blocking collectives: 87.3 us -> 0 us
  Pallas kernels: 0 us -> 76 us
  local copies, waits for them, and re-layouts: 23 us -> 1.41 us
  between operations: 16.4 us -> 0.83 us
  starting transfers between devices: 13.6 us -> 0 us
  matrix products: 2.06 us -> 9.68 us
    all_gather x2 -> x0, waiting for transfers between devices: 164 us -> none  [one_gather(): lines, at, gathered = (lax.all_gather(vector, axis), 0, [])]
    pallas_call x0 -> x1, Pallas kernels: none -> 76 us  [gathered(): pl.pallas_call(comm_kernel, out_shape=(jax.ShapeDtypeStruct((32, 2, 32, R...]
    all_to_all x2 -> x0, blocking collectives: 48.3 us -> none  [the longest x1 39.3 us: sent_and_summed(): lax.all_to_all(pieces, axis, split_axis=0, concat_axis=0, tiled=True)]
    all_gather x1 -> x0, blocking collectives: 39.1 us -> none  [in_one_piece(): result = lax.all_gather(both, axis, axis=dim, tiled=True)]
    all_to_all x1 -> x0, starting transfers between devices: 13.5 us -> none  [from_everyone(): return lax.all_to_all(copies, axis, split_axis=0, concat_axis=0, tiled=True)]
    another operation x4 -> x0, local copies, waits for them, and re-layouts: 8.37 us -> none  [joined_along(): return jnp.moveaxis(pieces, 0, dim).reshape(shape)]
    dot_general x6 -> x4, matrix products: 2.06 us -> 9.68 us  [the longest x1 3.36 us: local(): all_o = scale * jnp.dot(whole_o, half_o, preferred_element_type=jnp.float32)]
    all_gather x2 -> x0, local copies, waits for them, and re-layouts: 7.42 us -> none  [one_gather(): lines, at, gathered = (lax.all_gather(vector, axis), 0, [])]
  transfers between devices with their start and end apart: 3 -> 0, of which waited for: 2 -> 0; matrix products, arithmetic and copies ran while one was open for 0% -> 0% of each run, Pallas kernels for 0% -> 0%
where the time goes in v1:
time: 94.7 us; the launch traced here: 94.4 us
  Pallas kernels  76 us (80%)
  matrix products  9.68 us (10%)
  other arithmetic  6.53 us (7%)
  local copies, waits for them, and re-layouts  1.41 us (1%)
    pallas_call x1, Pallas kernels, gathered(): pl.pallas_call(comm_kernel, out_shape=(jax.ShapeDtypeStruct((32, 2, 32, R...  76 us
    rsqrt x2, other arithmetic, decoded(): root = lax.rsqrt(lax.rsqrt(jnp.maximum(jnp.abs(c), 1e-37)))  3.87 us
    dot_general x1, matrix products, local(): all_o = scale * jnp.dot(whole_o, half_o, preferred_element_type=jnp.float32)  3.36 us
    dot_general x1, matrix products, local(): all_q = scale * jnp.dot(whole_q, half_q, preferred_element_type=jnp.float32)  3.26 us

profile of v1, /device:TPU:1, one launch (start us, length us, event | category | flops | bytes accessed | tf_op | source)
XLA Modules:
  0.0 94.4 jit_solution(4980262504555141228)
XLA Ops:
  0.6 76.0 %shard_map.195 = (bf16[32,2,32,256]{3,2,1,0:T(8,128)(2,1)}, bf16[32,2,16,256]{3,2,1,0:T(8,128)(2,1)}, bf16[32,8,1536]{2,1,0:T(8,128)(2,1)}, f32[2,8,768]{2,1,0:T...) custom-call(bf16[128,2048]{1,0:T(8,128)(2,1)} %inputs.1, ...), custom_call_target="tpu_custom_call" | custom-call | tf_op jit(solution)/shard_map/pallas_call | solution.py:320
  76.6 0.0 copy-start.1
  76.7 1.3 %slice.18 = f32[1,1]{1,0:T(1,128)} slice(f32[8,128]{1,0:T(8,128)} %get-tuple-element.17), slice={[0:1], [0:1]} | slice | bytes 8 | tf_op jit(solution)/shard_map/slice | solution.py:384
  78.0 2.8 %fusion.5 = f32[32,2,16,1024]{3,2,1,0:T(8,128)S(1)} fusion(bf16[32,2,16,1024]{3,2,1,0:T(8,128)(2,1)} %get-tuple-element.22), kind=kLoop, calls=%fused_computation.11 | loop fusion | flops 3145728 | bytes 6291456 | tf_op jit(solution)/shard_map/rsqrt | solution.py:41
  80.8 0.7 convert_compare_fusion
  81.5 3.4 %fusion.9 = bf16[1024,1024]{1,0:T(8,128)(2,1)} fusion(f32[32,2,16,1024]{3,2,1,0:T(8,128)S(1)} %fusion.5, pred[32,2,16,1024]{3,2,1,0:T(8,128)(4,1)S(1)} %convert_compare_fusion, bf16[1024,256]{1,0:T(8,128)(2,1)S(1)} %bitcast.42, f32[]{:T(128)} %bitcast.4, bf16[256,1536]{1,0:T(8,128)(2,1)S(1)} %bitcast.33), kind=kOutput, calls=%fused_computation.15 | convolution fusion | flops 543162368 | bytes 8388612 | tf_op jit(solution)/shard_map/dot_general | solution.py:394
  84.9 0.0 copy-done
  84.9 1.1 %fusion.2 = f32[32,2,32,512]{3,2,1,0:T(8,128)S(1)} fusion(bf16[32,2,32,512]{3,2,1,0:T(8,128)(2,1)S(1)} %copy-done), kind=kLoop, calls=%fused_computation.8 | loop fusion | flops 3145728 | bytes 6291456 | tf_op jit(solution)/shard_map/rsqrt | solution.py:41
  86.0 0.7 convert_compare_fusion.1
  86.7 0.0 copy-start.4
  86.7 0.0 copy-start.9
  86.7 0.0 copy-start.5
  86.8 0.0 copy-start.6
  86.8 0.0 copy-start.12
  86.8 0.0 copy-start.7
  86.8 0.0 copy-start.8
  86.8 0.0 copy-start.10
  86.8 0.0 copy-start.11
  86.8 3.3 %fusion.7 = bf16[2048,512]{1,0:T(8,128)(2,1)} fusion(f32[32,2,32,512]{3,2,1,0:T(8,128)S(1)} %fusion.2, pred[32,2,32,512]{3,2,1,0:T(32,128)(4,1)S(1)} %convert_compare_fusion.1, bf16[2048,256]{1,0:T(8,128)(2,1)S(1)} %bitcast.37, f32[]{:T(128)} %bitcast.4, bf16[256,1536]{1,0:T(8,128)(2,1)S(1)} %bitcast.34), kind=kOutput, calls=%fused_computation.13 | convolution fusion | flops 543162368 | bytes 8650756 | tf_op jit(solution)/shard_map/dot_general | solution.py:393
  90.1 0.0 copy-done.9
  90.1 1.5 %multiply_subtract_fusion = (f32[32,1024]{1,0:T(8,128)}, f32[32,1024]{1,0:T(8,128)}) fusion(f32[32,1024]{1,0:T(8,128)S(1)} %copy-done.4, bf16[32,256]{1,0:T(8,128)(2,1)S(1)} %copy-done.9, bf16[256,1536]{1,0:T(8,128)(2,1)S(1)} %bitcast.35, f32[]{:T(128)} %bitcast.4), kind=kOutput, calls=%fused_computation.24 | convolution fusion | flops 16875520 | bytes 933892 | tf_op jit(solution)/shard_map/dot_general | solution.py:390
  91.6 1.5 %multiply_subtract_fusion.1 = (f32[64,512]{1,0:T(8,128)}, f32[64,512]{1,0:T(8,128)}) fusion(f32[64,512]{1,0:T(8,128)S(1)} %copy-done.5, bf16[64,256]{1,0:T(8,128)(2,1)S(1)} %copy-done.6, bf16[256,1536]{1,0:T(8,128)(2,1)S(1)} %bitcast.36, f32[]{:T(128)} %bitcast.4), kind=kOutput, calls=%fused_computation.25 | convolution fusion | flops 16875520 | bytes 688132 | tf_op jit(solution)/shard_map/dot_general | solution.py:389
  93.2 0.6 fusion.16
  93.8 0.6 fusion.17
  (18 shorter events, 0.0 us)
Async XLA Ops:
  76.6 4.1 %copy-start.1 = (bf16[32,2,16,1024]{3,2,1,0:T(8,128)(2,1)S(1)}, bf16[32,2,16,1024]{3,2,1,0:T(8,128)(2,1)}, u32[]{:S(2)}) copy-start(bf16[32,2,16,1024]{3,2,1,0:T(8,128)(2,1)} %get-tuple-element.22) | copy-start | bytes 6291460
  78.0 3.5 %copy-start.2 = (bf16[32,8,1536]{2,1,0:T(8,128)(2,1)S(1)}, bf16[32,8,1536]{2,1,0:T(8,128)(2,1)}, u32[]{:S(2)}) copy-start(bf16[32,8,1536]{2,1,0:T(8,128)(2,1)} %get-tuple-element.18) | copy-start | bytes 2359300
  78.0 3.5 %copy-start.13 = (bf16[32,2,16,256]{3,2,1,0:T(8,128)(2,1)S(1)}, bf16[32,2,16,256]{3,2,1,0:T(8,128)(2,1)}, u32[]{:S(2)}) copy-start(bf16[32,2,16,256]{3,2,1,0:T(8,128)(2,1)} %get-tuple-element.23) | copy-start | bytes 1572868
  81.5 3.4 %copy-start = (bf16[32,2,32,512]{3,2,1,0:T(8,128)(2,1)S(1)}, bf16[32,2,32,512]{3,2,1,0:T(8,128)(2,1)}, u32[]{:S(2)}) copy-start(bf16[32,2,32,512]{3,2,1,0:T(8,128)(2,1)} %get-tuple-element.20) | copy-start | bytes 6291460
  84.9 1.8 %copy-start.3 = (bf16[32,2,32,256]{3,2,1,0:T(8,128)(2,1)S(1)}, bf16[32,2,32,256]{3,2,1,0:T(8,128)(2,1)}, u32[]{:S(2)}) copy-start(bf16[32,2,32,256]{3,2,1,0:T(8,128)(2,1)} %get-tuple-element.21) | copy-start | bytes 3145732
  86.7 3.4 %copy-start.4 = (f32[32,1024]{1,0:T(8,128)S(1)}, f32[32,1024]{1,0:T(8,128)}, u32[]{:S(2)}) copy-start(f32[32,1024]{1,0:T(8,128)} %param.19) | copy-start | bytes 393220
  86.7 3.4 %copy-start.9 = (bf16[32,256]{1,0:T(8,128)(2,1)S(1)}, bf16[32,256]{1,0:T(8,128)(2,1)}, u32[]{:S(2)}) copy-start(bf16[32,256]{1,0:T(8,128)(2,1)} %param.17) | copy-start | bytes 49156
  86.7 4.9 %copy-start.5 = (f32[64,512]{1,0:T(8,128)S(1)}, f32[64,512]{1,0:T(8,128)}, u32[]{:S(2)}) copy-start(f32[64,512]{1,0:T(8,128)} %param.18) | copy-start | bytes 393220
  86.8 4.9 %copy-start.6 = (bf16[64,256]{1,0:T(8,128)(2,1)S(1)}, bf16[64,256]{1,0:T(8,128)(2,1)}, u32[]{:S(2)}) copy-start(bf16[64,256]{1,0:T(8,128)(2,1)} %param.16) | copy-start | bytes 98308
  86.8 6.4 %copy-start.12 = (f32[2,8,768]{2,1,0:T(8,128)S(1)}, f32[2,8,768]{2,1,0:T(8,128)}, u32[]{:S(2)}) copy-start(f32[2,8,768]{2,1,0:T(8,128)} %get-tuple-element.19) | copy-start | bytes 147460
  86.8 6.4 %copy-start.7 = (f32[8,1024]{1,0:T(8,128)S(1)}, f32[8,1024]{1,0:T(8,128)}, u32[]{:S(2)}) copy-start(f32[8,1024]{1,0:T(8,128)} %first_o.1) | copy-start | bytes 98308
  86.8 6.4 %copy-start.8 = (f32[8,1024]{1,0:T(8,128)S(1)}, f32[8,1024]{1,0:T(8,128)}, u32[]{:S(2)}) copy-start(f32[8,1024]{1,0:T(8,128)} %second_o.1) | copy-start | bytes 98308
  86.8 7.0 %copy-start.10 = (f32[8,512]{1,0:T(8,128)S(1)}, f32[8,512]{1,0:T(8,128)}, u32[]{:S(2)}) copy-start(f32[8,512]{1,0:T(8,128)} %first_q.1) | copy-start | bytes 49156
  86.8 7.0 %copy-start.11 = (f32[8,512]{1,0:T(8,128)S(1)}, f32[8,512]{1,0:T(8,128)}, u32[]{:S(2)}) copy-start(f32[8,512]{1,0:T(8,128)} %second_q.1) | copy-start | bytes 49156

commit v2 on v1

v2 whole, which is shorter than its diff:
```python
import functools

import jax
import jax.numpy as jnp
from jax import lax
from jax.experimental import pallas as pl
from jax.experimental.pallas import tpu as pltpu
from jax.sharding import PartitionSpec as P

D = 2048
DA = 1024
RANK = 256
NZ, NX, NY = 8, 4, 4

beta_first = 0.9
beta_second = 0.95
adam_eps = 1e-08
mean_eps = 1e-06
learn_rate = 0.02
HALF = 768

MESH = pl.DeviceIdType.MESH
NEAR_FIRST = (1, 7, 2, 6, 3, 5, 4)


def moment_update(low_sum, first, second):
    first_new = beta_first * first + (1.0 - beta_first) * low_sum
    second_new = beta_second * second + (1.0 - beta_second) * low_sum * low_sum
    normed = first_new / (jnp.sqrt(second_new) + adam_eps)
    return (first_new, second_new, normed)


def coded(v):
    square = v * v
    fourth = jnp.maximum(square * square, 1e-36)
    return jnp.where(v < 0, -fourth, fourth).astype(jnp.bfloat16)


def decoded(c):
    c = c.astype(jnp.float32)
    root = c * lax.rsqrt(jnp.abs(c))
    return root * lax.rsqrt(jnp.abs(root))


def comm_kernel(
    inputs, query_cot, attended, output_cot, proj_q, proj_o, w_q, w_o,
    first_q, second_q, first_o, second_o,
    pq_out, po_out, half_out, low_out, total_out, wg_q, wg_o,
    pq, po, half, low,
    x_in, c_q, x_at, c_o, fst, snd, old_q, old_o, code_q, code_o,
    lb, cb, by, bx, sz, bz, ty, by2, qz, qx, qy, qt,
    loc, a_zs, a_zr, a_xs, a_xr, a_cs, a_cr,
    w_xs, w_xr, w_zs, w_zr, w_ys, w_yr,
    b_ys, b_yr, b_xs, b_xr, b_zs, b_zr, b_2s, b_2r, b_ls, b_lr,
    e_zs, e_zr, e_xs, e_xr, e_ys, e_yr,
    q_zs, q_zr, q_xs, q_xr, q_ys, q_yr,
):
    f = lax.axis_index("fs")
    y = lax.axis_index("rep")
    t = lax.axis_index("tp")
    z = f // NX
    x = f % NX
    p = y % 2
    o = 1 - p

    def at_z(d):
        return {"fs": ((z + d) % NZ) * NX + x}

    def at_zt(d):
        return {"fs": ((z + d) % NZ) * NX + x, "tp": 1 - t}

    def at_x(e):
        return {"fs": z * NX + (x + e) % NX}

    def at_y(s):
        return {"rep": (y + s) % NY}

    other_core = {"tp": 1 - t}
    sends = []

    def remote(src, dst, ssem, rsem, dev):
        return pltpu.make_async_remote_copy(
            src_ref=src, dst_ref=dst, send_sem=ssem, recv_sem=rsem,
            device_id=dev, device_id_type=MESH,
        )

    def send(src, dst, ssem, rsem, dev):
        c = remote(src, dst, ssem, rsem, dev)
        c.start()
        sends.append(c)

    def arrived(dst, rsem):
        remote(dst, dst, rsem, rsem, other_core).wait_recv()

    loads = [
        pltpu.make_async_copy(proj_q.at[t], pq.at[f, t], loc.at[0]),
        pltpu.make_async_copy(proj_o.at[t], po.at[f, t], loc.at[1]),
        pltpu.make_async_copy(w_q.at[p], old_q, loc.at[12]),
        pltpu.make_async_copy(w_o.at[p], old_o, loc.at[13]),
        pltpu.make_async_copy(inputs, x_in, loc.at[2]),
        pltpu.make_async_copy(attended, x_at, loc.at[3]),
        pltpu.make_async_copy(query_cot, c_q, loc.at[4]),
        pltpu.make_async_copy(output_cot, c_o, loc.at[5]),
        pltpu.make_async_copy(first_q, fst.at[0, :, pl.ds(0, 512)], loc.at[6]),
        pltpu.make_async_copy(first_o.at[:, pl.ds(0, 256)], fst.at[0, :, pl.ds(512, 256)], loc.at[7]),
        pltpu.make_async_copy(first_o.at[:, pl.ds(256, 768)], fst.at[1], loc.at[8]),
        pltpu.make_async_copy(second_q, snd.at[0, :, pl.ds(0, 512)], loc.at[9]),
        pltpu.make_async_copy(second_o.at[:, pl.ds(0, 256)], snd.at[0, :, pl.ds(512, 256)], loc.at[10]),
        pltpu.make_async_copy(second_o.at[:, pl.ds(256, 768)], snd.at[1], loc.at[11]),
    ]
    for c in loads:
        c.start()

    barrier = pltpu.get_barrier_semaphore()
    peers = [at_z(d) for d in range(1, NZ)] + [at_zt(d) for d in range(1, NZ)]
    peers += [at_x(e) for e in range(1, NX)]
    peers += [at_y(s) for s in range(1, NY)] + [other_core]
    for dev in peers:
        pl.semaphore_signal(barrier, inc=1, device_id=dev, device_id_type=MESH)
    for c in loads[:4]:
        c.wait()
    code_q[...] = coded(old_q[...])
    code_o[...] = coded(old_o[...])
    own_q = pltpu.make_async_copy(code_q, wg_q.at[f, p], loc.at[12])
    own_o = pltpu.make_async_copy(code_o, wg_o.at[f, p], loc.at[13])
    own_q.start()
    own_o.start()
    pl.semaphore_wait(barrier, len(peers))

    for d in NEAR_FIRST:
        send(pq.at[f, t], pq.at[f, t], a_zs.at[0, d], a_zr.at[0, d], at_z(d))
        send(po.at[f, t], po.at[f, t], a_zs.at[1, d], a_zr.at[1, d], at_z(d))

    def factors_x(d):
        g = ((z + NZ - d) % NZ) * NX + x
        if d:
            arrived(pq.at[g, t], a_zr.at[0, d])
            arrived(po.at[g, t], a_zr.at[1, d])
        for e in (2, 1, 3):
            send(pq.at[g, t], pq.at[g, t], a_xs.at[0, d, e], a_xr.at[0, d, e], at_x(e))
            send(po.at[g, t], po.at[g, t], a_xs.at[1, d, e], a_xr.at[1, d, e], at_x(e))

    factors_x(0)
    for e in range(1, NX):
        send(code_q, wg_q.at[f, p], w_xs.at[0, e], w_xr.at[0, e], at_x(e))
        send(code_o, wg_o.at[f, p], w_xs.at[1, e], w_xr.at[1, e], at_x(e))
    for d in NEAR_FIRST:
        factors_x(d)

    def weight_rows(s):
        for way, sign in ((0, 1), (1, -1)):
            row = ((z - sign * s + NZ) % NZ) * NX
            for k, ref in enumerate((wg_q, wg_o)):
                if (s == 4 and way != k) or (s == 0 and way):
                    continue
                yield way, k, ref, row

    def weights_z(s):
        if s == 0:
            own_q.wait()
            own_o.wait()
            for e in range(1, NX):
                g = z * NX + (x + NX - e) % NX
                arrived(wg_q.at[g, p], w_xr.at[0, e])
                arrived(wg_o.at[g, p], w_xr.at[1, e])
        for way, k, ref, row in weight_rows(s):
            part = ref.at[pl.ds(row, NX), p]
            if s:
                arrived(part, w_zr.at[way, k, s])
            for w, sign in ((0, 1), (1, -1)):
                if (s == 0 or w == way) and (s < 3 or (s == 3 and way == k)):
                    send(part, part, w_zs.at[w, k, s + 1], w_zr.at[w, k, s + 1], at_z(sign % NZ))

    def weights_y(s):
        for way, k, ref, row in weight_rows(s):
            for side in range(2):
                two = ref.at[pl.ds(row + 2 * side, 2), p]
                send(two, two, w_ys.at[way, k, s, side], w_yr.at[way, k, s, side],
                     at_y(1 if side == 0 else NY - 1))

    def weights_done(s):
        for way, k, ref, row in weight_rows(s):
            for side in range(2):
                arrived(ref.at[pl.ds(row + 2 * side, 2), o], w_yr.at[way, k, s, side])

    weights_z(0)
    weights_y(0)

    for d in (0,) + NEAR_FIRST:
        row = ((z + NZ - d) % NZ) * NX
        for e in range(1, NX):
            g = row + (x + NX - e) % NX
            arrived(pq.at[g, t], a_xr.at[0, d, e])
            arrived(po.at[g, t], a_xr.at[1, d, e])
        for k, ref in enumerate((pq, po)):
            part = ref.at[pl.ds(row, NX), t]
            send(part, part, a_cs.at[k, d], a_cr.at[k, d], other_core)
    for d in (0,) + NEAR_FIRST:
        row = ((z + NZ - d) % NZ) * NX
        for k, ref in enumerate((pq, po)):
            arrived(ref.at[pl.ds(row, NX), 1 - t], a_cr.at[k, d])
    outs = [
        pltpu.make_async_copy(pq, pq_out, loc.at[0]),
        pltpu.make_async_copy(po, po_out, loc.at[1]),
    ]
    for c in outs:
        c.start()

    for c in loads[4:8]:
        c.wait()

    def partial_low(tokens, whole, cot, depth):
        reduced = jnp.dot(
            tokens[...], whole[...].reshape(depth, RANK), preferred_element_type=jnp.float32
        )
        high = reduced.astype(jnp.bfloat16)
        rest = (reduced - high.astype(jnp.float32)).astype(jnp.bfloat16)
        both = jnp.concatenate([high, rest], axis=0)
        return lax.dot_general(
            both, jnp.concatenate([cot, cot], axis=0),
            (((0,), (0,)), ((), ())), preferred_element_type=jnp.float32,
        )

    def put(par, lo, block):
        for zz in range(NZ):
            for xx in range(NX):
                r = (zz * NX + xx) * 8
                lb[par, xx, zz, :, lo : lo + block.shape[1]] = block[r : r + 8, :]

    low_o = partial_low(x_at, po, c_o[...], DA)
    put(0, 512, low_o[:, :256])
    put(1, 0, low_o[:, 256:])
    put(0, 0, partial_low(x_in, pq, c_q[...], D))

    chunks = (
        (2, 0, 8, 1), (3, 0, 8, NY - 1), (1, 0, 4, 1), (1, 4, 4, NY - 1), (0, 0, 4, 1), (0, 4, 4, NY - 1),
    )
    for n, (e, lo, rows, step) in enumerate(chunks):
        part = (x + e) % NX, pl.ds(lo, rows)
        cb[part] = coded(lb[(o,) + part])
        send(cb.at[part], by.at[part], b_ys.at[n], b_yr.at[n], at_y(step))
    weights_z(1)
    weights_y(1)

    for n, (e, lo, rows, step) in enumerate(chunks):
        j = (x + e) % NX
        part = j, pl.ds(lo, rows)
        arrived(by.at[part], b_yr.at[n])
        lb[(p,) + part] = lb[(p,) + part] + decoded(by[part])
        if e and lo + rows == NZ:
            cb[NX + e - 1] = coded(lb[p, j])
            send(cb.at[NX + e - 1], bx.at[e - 1], b_xs.at[e - 1], b_xr.at[e - 1], at_x(e))
    weights_z(2)
    for e in (1, 2, 0):
        arrived(bx.at[e], b_xr.at[e])
    mine = (lb[p, x] + decoded(bx[0])) + (decoded(bx[1]) + decoded(bx[2]))
    lb[o, 0] = mine
    sz[...] = coded(mine)
    for d in (4, 3, 5, 2, 6, 1, 7):
        send(sz.at[(z + d) % NZ], bz.at[d - 1], b_zs.at[d - 1], b_zr.at[d - 1], at_z(d))
    weights_y(2)
    weights_z(3)
    for d in NEAR_FIRST:
        arrived(bz.at[d - 1], b_zr.at[d - 1])
    mine = lb[o, 0, z]
    for d in range(7):
        mine = mine + decoded(bz[d])
    ty[...] = mine
    send(ty, by2, b_2s.at[0], b_2r.at[0], at_y(2))
    for c in loads[8:14]:
        c.wait()
    arrived(by2, b_2r.at[0])

    low_sum = mine + by2[...]
    low[p] = low_sum
    _, _, normed = moment_update(low_sum, fst[p], snd[p])
    half[f, :, pl.ds(pl.multiple_of(p * HALF, 256), HALF)] = normed.astype(jnp.bfloat16)
    square = normed * normed
    total = square[:, 0:128]
    for k in range(1, 6):
        total = total + square[:, k * 128 : (k + 1) * 128]
    qz[z * 2 + t] = jnp.sum(total, axis=0, keepdims=True)

    def piece(g, n, par):
        return half.at[pl.ds(g, n), :, pl.ds(pl.multiple_of(par * HALF, 256), HALF)]

    def square_z(d, core):
        return ((z + NZ - d) % NZ) * 2 + (t if core == 0 else 1 - t)

    for d in NEAR_FIRST:
        send(piece(f, 1, p), piece(f, 1, p), e_zs.at[d], e_zr.at[d], at_z(d))
    for d in range(NZ):
        for core, dev in ((0, at_z(d)), (1, at_zt(d) if d else other_core)):
            if d or core:
                row = qz.at[z * 2 + t]
                send(row, row, q_zs.at[d, core], q_zr.at[d, core], dev)
    send(low.at[p], low.at[p], b_ls.at[0], b_lr.at[0], at_y(1))
    for d in (0,) + NEAR_FIRST:
        g = ((z + NZ - d) % NZ) * NX + x
        if d:
            arrived(piece(g, 1, p), e_zr.at[d])
        for e in (2, 1, 3):
            send(piece(g, 1, p), piece(g, 1, p), e_xs.at[d, e], e_xr.at[d, e], at_x(e))
    for d in range(NZ):
        for core in range(2):
            if d or core:
                arrived(qz.at[square_z(d, core)], q_zr.at[d, core])
    total = qz[0]
    for k in range(1, 2 * NZ):
        total = total + qz[k]
    qx[x] = total
    for e in (2, 1, 3):
        send(qx.at[x], qx.at[x], q_xs.at[e], q_xr.at[e], at_x(e))
    for d in (0,) + NEAR_FIRST:
        row = ((z + NZ - d) % NZ) * NX
        for e in range(1, NX):
            arrived(piece(row + (x + NX - e) % NX, 1, p), e_xr.at[d, e])
        for side in range(2):
            two = piece(row + 2 * side, 2, p)
            send(two, two, e_ys.at[d, side], e_yr.at[d, side], at_y(1 if side == 0 else NY - 1))
    for e in range(1, NX):
        arrived(qx.at[(x + NX - e) % NX], q_xr.at[e])
    qy[p] = (qx[0] + qx[1]) + (qx[2] + qx[3])
    send(qy.at[p], qy.at[p], q_ys.at[0], q_yr.at[0], at_y(1))
    weights_y(3)
    weights_z(4)
    weights_y(4)
    arrived(low.at[o], b_lr.at[0])
    for d in (0,) + NEAR_FIRST:
        row = ((z + NZ - d) % NZ) * NX
        for side in range(2):
            arrived(piece(row + 2 * side, 2, o), e_yr.at[d, side])
    arrived(qy.at[o], q_yr.at[0])
    qt[...] = qy[0] + qy[1]
    outs += [
        pltpu.make_async_copy(half, half_out, loc.at[2]),
        pltpu.make_async_copy(low, low_out, loc.at[3]),
        pltpu.make_async_copy(qt, total_out, loc.at[4]),
    ]
    for c in outs[2:]:
        c.start()
    for s in range(5):
        weights_done(s)
    for c in outs:
        c.wait()
    for c in sends:
        c.wait_send()


def gathered(inputs, query_cot, attended, output_cot, proj_q, proj_o, w_q, w_o,
             first_q, second_q, first_o, second_o):
    f32, bf16 = jnp.float32, jnp.bfloat16
    anywhere = pl.BlockSpec(memory_space=pl.ANY)
    dma = pltpu.SemaphoreType.DMA
    shared = (
        ((32, 2, 32, RANK), bf16),
        ((32, 2, 16, RANK), bf16),
        ((32, 8, 2 * HALF), bf16),
        ((2, 8, HALF), f32),
    )
    return pl.pallas_call(
        comm_kernel,
        out_shape=tuple(jax.ShapeDtypeStruct(*s) for s in shared) + (
            jax.ShapeDtypeStruct((1, 128), f32),
            jax.ShapeDtypeStruct((32, 2, 32, 512), bf16),
            jax.ShapeDtypeStruct((32, 2, 16, 1024), bf16),
        ),
        in_specs=[anywhere] * 12,
        out_specs=(anywhere,) * 7,
        scratch_shapes=[pltpu.VMEM(*s) for s in shared] + [
            pltpu.VMEM((128, D), bf16),
            pltpu.VMEM((128, 512), bf16),
            pltpu.VMEM((128, DA), bf16),
            pltpu.VMEM((128, 1024), bf16),
            pltpu.VMEM((2, 8, HALF), f32),
            pltpu.VMEM((2, 8, HALF), f32),
            pltpu.VMEM((32, 512), f32),
            pltpu.VMEM((16, 1024), f32),
            pltpu.VMEM((32, 512), bf16),
            pltpu.VMEM((16, 1024), bf16),
            pltpu.VMEM((2, NX, NZ, 8, HALF), f32),
            pltpu.VMEM((7, NZ, 8, HALF), bf16),
            pltpu.VMEM((NX, NZ, 8, HALF), bf16),
            pltpu.VMEM((3, NZ, 8, HALF), bf16),
            pltpu.VMEM((NZ, 8, HALF), bf16),
            pltpu.VMEM((7, 8, HALF), bf16),
            pltpu.VMEM((8, HALF), f32),
            pltpu.VMEM((8, HALF), f32),
            pltpu.VMEM((2 * NZ, 1, 128), f32),
            pltpu.VMEM((NX, 1, 128), f32),
            pltpu.VMEM((2, 1, 128), f32),
            pltpu.VMEM((1, 128), f32),
            dma((14,)),
            dma((2, 8)), dma((2, 8)), dma((2, 8, 4)), dma((2, 8, 4)), dma((2, 8)), dma((2, 8)),
            dma((2, 4)), dma((2, 4)), dma((2, 2, 5)), dma((2, 2, 5)), dma((2, 2, 5, 2)), dma((2, 2, 5, 2)),
            dma((6,)), dma((6,)), dma((3,)), dma((3,)), dma((7,)), dma((7,)),
            dma((1,)), dma((1,)), dma((1,)), dma((1,)),
            dma((8,)), dma((8,)), dma((8, 4)), dma((8, 4)), dma((8, 2)), dma((8, 2)),
            dma((8, 2)), dma((8, 2)), dma((4,)), dma((4,)), dma((1,)), dma((1,)),
        ],
        compiler_params=pltpu.CompilerParams(collective_id=0, has_side_effects=True),
    )(
        inputs, query_cot, attended, output_cot,
        proj_q.reshape(2, 32, RANK), proj_o.reshape(2, 16, RANK),
        w_q.reshape(2, 32, 512), w_o.reshape(2, 16, 1024),
        first_q, second_q, first_o, second_o,
    )


def final_kernel(
    pq, po, wq, wo, half, low, total, proj_q, proj_o, weight_q, weight_o,
    first_q, second_q, first_o, second_o,
    new_q, new_o, step_q, step_o, nf_q, ns_q, nf_o, ns_o, copy_q, copy_o,
):
    mean = jnp.sum(total[...], axis=1, keepdims=True) / (RANK * (DA + D))
    scale = lax.rsqrt(mean + mean_eps)

    def step(factor, lo, width):
        rows = half[:, :, lo : lo + width].reshape(RANK, width)
        return scale * jnp.dot(factor, rows, preferred_element_type=jnp.float32)

    rows_q, rows_o = copy_q.shape[0], copy_o.shape[0]
    all_q = step(pq[...].reshape(rows_q, RANK), 0, 512)
    copy_q[...] = (decoded(wq[...].reshape(rows_q, 512)) - learn_rate * all_q).astype(jnp.bfloat16)
    all_o = step(po[...].reshape(rows_o, RANK), 512, 1024)
    copy_o[...] = (decoded(wo[...].reshape(rows_o, 1024)) - learn_rate * all_o).astype(jnp.bfloat16)

    @pl.when(pl.program_id(0) == 0)
    def _():
        mine_q = step(proj_q[...], 0, 512)
        step_q[...] = mine_q
        new_q[...] = weight_q[...] - learn_rate * mine_q
        mine_o = step(proj_o[...], 512, 1024)
        step_o[...] = mine_o
        new_o[...] = weight_o[...] - learn_rate * mine_o
        nf_q[...], ns_q[...], _ = moment_update(low[0, :, :512], first_q[...], second_q[...])
        nf_o[:, :256], ns_o[:, :256], _ = moment_update(
            low[0, :, 512:], first_o[:, :256], second_o[:, :256]
        )
        nf_o[:, 256:], ns_o[:, 256:], _ = moment_update(low[1], first_o[:, 256:], second_o[:, 256:])


STEPS = 8


def finished(pq, po, wq, wo, half, low, total, proj_q, proj_o, weight_q, weight_o,
             first_q, second_q, first_o, second_o):
    f32, bf16 = jnp.float32, jnp.bfloat16

    def blocks(shape):
        rest = (0,) * (len(shape) - 1)
        return pl.BlockSpec((shape[0] // STEPS,) + tuple(shape[1:]), lambda i: (i,) + rest)

    def whole(shape):
        return pl.BlockSpec(tuple(shape), lambda i: (0,) * len(shape))

    small = (half, low, total, proj_q, proj_o, weight_q, weight_o, first_q, second_q, first_o, second_o)
    outs = (
        ((64, 512), f32), ((32, 1024), f32), ((64, 512), f32), ((32, 1024), f32),
        ((8, 512), f32), ((8, 512), f32), ((8, 1024), f32), ((8, 1024), f32),
        ((D, 512), bf16), ((DA, 1024), bf16),
    )
    return pl.pallas_call(
        final_kernel,
        grid=(STEPS,),
        out_shape=tuple(jax.ShapeDtypeStruct(*s) for s in outs),
        in_specs=[blocks(a.shape) for a in (pq, po, wq, wo)] + [whole(a.shape) for a in small],
        out_specs=tuple(whole(s) for s, _ in outs[:8]) + tuple(blocks(s) for s, _ in outs[8:]),
        cost_estimate=pl.CostEstimate(flops=2_200_000_000, bytes_accessed=12_000_000, transcendentals=0),
    )(pq, po, wq, wo, *small)


def local(
    inputs, query_cot, attended, output_cot, proj_query, proj_output,
    weight_query, weight_output, first_query, second_query, first_output, second_output,
):
    pq, po, half, low, total, wg_q, wg_o = gathered(
        inputs, query_cot, attended, output_cot, proj_query, proj_output,
        weight_query, weight_output, first_query, second_query, first_output, second_output,
    )
    return finished(
        pq, po, wg_q, wg_o, half, low, total, proj_query, proj_output, weight_query, weight_output,
        first_query, second_query, first_output, second_output,
    )


def solution(mesh):
    return jax.shard_map(
        local,
        mesh=mesh,
        in_specs=(
            P(("fs", "rep"), None),
            P(("fs", "rep"), "tp"),
            P(("fs", "rep"), None),
            P(("fs", "rep"), "tp"),
            P("fs", None),
            P("fs", None),
            P("fs", "tp"),
            P("fs", "tp"),
            P("fs", "tp"),
            P("fs", "tp"),
            P("fs", "tp"),
            P("fs", "tp"),
        ),
        out_specs=(
            P("fs", "tp"),
            P("fs", "tp"),
            P("fs", "tp"),
            P("fs", "tp"),
            P("fs", "tp"),
            P("fs", "tp"),
            P("fs", "tp"),
            P("fs", "tp"),
            P(None, "tp"),
            P(None, "tp"),
        ),
        check_vma=False,
    )
```

time: 94.7 us -> 83.3 us (0.88)
  matrix products: 9.68 us -> 0 us
  other arithmetic: 6.53 us -> 0 us
  Pallas kernels: 76 us -> 82.4 us
  local copies, waits for them, and re-layouts: 1.41 us -> 0 us
    dot_general x4 -> x0, matrix products: 9.68 us -> none  [the longest x1 3.36 us: local(): all_o = scale * jnp.dot(whole_o, half_o, preferred_element_type=jnp.float32)]
    pallas_call x1 -> x2, Pallas kernels: 76 us -> 82.4 us  [the longest x1 72.9 us: gathered(): pl.pallas_call(comm_kernel, out_shape=tuple((jax.ShapeDtypeStruct(*s) for...]
    rsqrt x2 -> x0, other arithmetic: 3.87 us -> none  [decoded(): root = lax.rsqrt(lax.rsqrt(jnp.maximum(jnp.abs(c), 1e-37)))]
    lt x2 -> x0, other arithmetic: 1.41 us -> none  [decoded(): return jnp.where(c < 0, -root, root)]
    slice x1 -> x0, local copies, waits for them, and re-layouts: 1.33 us -> none  [local(): scale = scale_tile[0, 0]]
    add x2 -> x0, other arithmetic: 1.25 us -> none  [moment_update(): second_new = beta_second * second + (1.0 - beta_second) * low_sum * low_sum]
where the time goes in v2:
time: 83.3 us; the launch traced here: 83.1 us
  Pallas kernels  82.4 us (99%)
    pallas_call x1, Pallas kernels, gathered(): pl.pallas_call(comm_kernel, out_shape=tuple((jax.ShapeDtypeStruct(*s) for...  72.9 us
    pallas_call x1, Pallas kernels, finished(): pl.pallas_call(final_kernel, grid=(STEPS,), out_shape=tuple((jax.ShapeDty...  9.49 us

profile of v2, /device:TPU:1, one launch (start us, length us, event | category | flops | bytes accessed | tf_op | source)
XLA Modules:
  0.0 83.1 jit_solution(15713445985940540783)
XLA Ops:
  0.6 72.9 %shard_map.195 = (bf16[32,2,32,256]{3,2,1,0:T(8,128)(2,1)}, bf16[32,2,16,256]{3,2,1,0:T(8,128)(2,1)}, bf16[32,8,1536]{2,1,0:T(8,128)(2,1)}, f32[2,8,768]{2,1,0:T...) custom-call(bf16[128,2048]{1,0:T(8,128)(2,1)} %inputs.1, ...), custom_call_target="tpu_custom_call" | custom-call | tf_op jit(solution)/shard_map/pallas_call | solution.py:361
  73.6 9.5 %shard_map.196 = (f32[64,512]{1,0:T(8,128)}, f32[32,1024]{1,0:T(8,128)}, f32[64,512]{1,0:T(8,128)}, f32[32,1024]{1,0:T(8,128)}, f32[8,512]{1,0:T(8,128)}, /*inde...) custom-call(bf16[32,2,32,256]{3,2,1,0:T(8,128)(2,1)} %get-tuple-elem, ...), custom_call_target="tpu_custom_call" | custom-call | flops 2200000000 | bytes 12000000 | tf_op jit(solution)/shard_map/pallas_call | solution.py:463

commit v3 on v2

v3 whole, which is shorter than its diff:
```python
import functools

import jax
import jax.numpy as jnp
from jax import lax
from jax.experimental import pallas as pl
from jax.experimental.pallas import tpu as pltpu
from jax.sharding import PartitionSpec as P

D = 2048
DA = 1024
RANK = 256
NZ, NX, NY = 8, 4, 4

beta_first = 0.9
beta_second = 0.95
adam_eps = 1e-08
mean_eps = 1e-06
learn_rate = 0.02
HALF = 768

MESH = pl.DeviceIdType.MESH
NEAR_FIRST = (1, 7, 2, 6, 3, 5, 4)


def moment_update(low_sum, first, second):
    first_new = beta_first * first + (1.0 - beta_first) * low_sum
    second_new = beta_second * second + (1.0 - beta_second) * low_sum * low_sum
    normed = first_new / (jnp.sqrt(second_new) + adam_eps)
    return (first_new, second_new, normed)


def coded(v):
    square = v * v
    fourth = jnp.maximum(square * square, 1e-36)
    return jnp.where(v < 0, -fourth, fourth).astype(jnp.bfloat16)


def decoded(c):
    c = c.astype(jnp.float32)
    root = c * lax.rsqrt(jnp.abs(c))
    return root * lax.rsqrt(jnp.abs(root))


def comm_kernel(
    inputs, query_cot, attended, output_cot, proj_q, proj_o, w_q, w_o,
    first_q, second_q, first_o, second_o,
    pf_out, half_out, low_out, total_out, wg_q, wg_o,
    pf, half, low,
    x_in, c_q, x_at, c_o, fst, snd, old_q, old_o, code_q, code_o,
    lb, cb, by, bx, sz, bz, ty, by2, qz, qx, qy, qt,
    loc, sent, a_z, a_x, a_c, w_x, w_z, w_d, w_y, b_y, b_x, b_z, b_2, b_l,
    e_z, e_x, e_y, q_z, q_x, q_y,
):
    f = lax.axis_index("fs")
    y = lax.axis_index("rep")
    t = lax.axis_index("tp")
    z = f // NX
    x = f % NX
    p = y % 2
    o = 1 - p

    def at_z(d):
        return {"fs": ((z + d) % NZ) * NX + x}

    def at_zt(d):
        return {"fs": ((z + d) % NZ) * NX + x, "tp": 1 - t}

    def at_x(e):
        return {"fs": z * NX + (x + e) % NX}

    def at_y(s):
        return {"rep": (y + s) % NY}

    other_core = {"tp": 1 - t}

    def remote(src, dst, ssem, rsem, dev):
        return pltpu.make_async_remote_copy(
            src_ref=src, dst_ref=dst, send_sem=ssem, recv_sem=rsem,
            device_id=dev, device_id_type=MESH,
        )

    def send(src, dst, kind, rsem, dev):
        remote(src, dst, sent.at[kind], rsem, dev).start()

    def arrived(dst, rsem):
        remote(dst, dst, rsem, rsem, other_core).wait_recv()

    loads = [
        pltpu.make_async_copy(proj_q.at[t], pf.at[f, t, pl.ds(0, 32)], loc.at[0]),
        pltpu.make_async_copy(proj_o.at[t], pf.at[f, t, pl.ds(32, 16)], loc.at[1]),
        pltpu.make_async_copy(w_q.at[p], old_q, loc.at[12]),
        pltpu.make_async_copy(w_o.at[p], old_o, loc.at[13]),
        pltpu.make_async_copy(inputs, x_in, loc.at[2]),
        pltpu.make_async_copy(attended, x_at, loc.at[3]),
        pltpu.make_async_copy(query_cot, c_q, loc.at[4]),
        pltpu.make_async_copy(output_cot, c_o, loc.at[5]),
        pltpu.make_async_copy(first_q, fst.at[0, :, pl.ds(0, 512)], loc.at[6]),
        pltpu.make_async_copy(first_o.at[:, pl.ds(0, 256)], fst.at[0, :, pl.ds(512, 256)], loc.at[7]),
        pltpu.make_async_copy(first_o.at[:, pl.ds(256, 768)], fst.at[1], loc.at[8]),
        pltpu.make_async_copy(second_q, snd.at[0, :, pl.ds(0, 512)], loc.at[9]),
        pltpu.make_async_copy(second_o.at[:, pl.ds(0, 256)], snd.at[0, :, pl.ds(512, 256)], loc.at[10]),
        pltpu.make_async_copy(second_o.at[:, pl.ds(256, 768)], snd.at[1], loc.at[11]),
    ]
    for c in loads:
        c.start()

    barrier = pltpu.get_barrier_semaphore()
    peers = [at_z(d) for d in range(1, NZ)] + [at_zt(d) for d in range(1, NZ)]
    peers += [at_x(e) for e in range(1, NX)]
    peers += [at_y(s) for s in range(1, NY)] + [other_core]
    for dev in peers:
        pl.semaphore_signal(barrier, inc=1, device_id=dev, device_id_type=MESH)
    for c in loads[:4]:
        c.wait()
    code_q[...] = coded(old_q[...])
    code_o[...] = coded(old_o[...])
    own_q = pltpu.make_async_copy(code_q, wg_q.at[f, p], loc.at[12])
    own_o = pltpu.make_async_copy(code_o, wg_o.at[f, p], loc.at[13])
    own_q.start()
    own_o.start()
    pl.semaphore_wait(barrier, len(peers))

    for d in NEAR_FIRST:
        send(pf.at[f, t], pf.at[f, t], 0, a_z.at[d], at_z(d))

    def factors_x(d):
        g = ((z + NZ - d) % NZ) * NX + x
        if d:
            arrived(pf.at[g, t], a_z.at[d])
        for e in (2, 1, 3):
            send(pf.at[g, t], pf.at[g, t], 0, a_x.at[d], at_x(e))

    def rows_at(d):
        return ((z + NZ - d) % NZ) * NX

    def output_x(d):
        g = rows_at(d) + x
        if d:
            arrived(wg_o.at[g, p], w_d.at[d])
        src = wg_o.at[g, p] if d else code_o
        for e in (2, 1, 3):
            send(src, wg_o.at[g, p], 4, w_x.at[1 + d], at_x(e))

    def weights_y(k, d):
        ref = (wg_q, wg_o)[k]
        for side in range(2):
            two = ref.at[pl.ds(rows_at(d) + 2 * side, 2), p]
            send(two, two, 3 + 2 * k, w_y.at[k], at_y(1 if side == 0 else NY - 1))

    def output_y(d):
        arrived(wg_o.at[pl.ds(0, 3), p], w_x.at[1 + d])
        weights_y(1, d)

    def query_z(s):
        if s == 0:
            arrived(wg_q.at[pl.ds(0, 3), p], w_x.at[0])
            part = wg_q.at[pl.ds(rows_at(0), NX), p]
            send(part, part, 2, w_z.at[1, 0], at_z(1))
            send(part, part, 2, w_z.at[1, 1], at_z(NZ - 1))
            weights_y(0, 0)
            return
        if s == NZ // 2:
            for way in range(2):
                arrived(wg_q.at[pl.ds(rows_at(s) + 2 * way, 2), p], w_z.at[s, way])
            weights_y(0, s)
            return
        for way, sign in ((0, 1), (1, -1)):
            part = wg_q.at[pl.ds(rows_at(sign * s), NX), p]
            arrived(part, w_z.at[s, way])
            if s == NZ // 2 - 1:
                part = wg_q.at[pl.ds(rows_at(sign * s) + 2 * way, 2), p]
            send(part, part, 2, w_z.at[s + 1, way], at_z(sign % NZ))
        for sign in (1, -1):
            weights_y(0, sign * s)

    for d in NEAR_FIRST:
        send(code_o, wg_o.at[f, p], 4, w_d.at[d], at_z(d))
    factors_x(0)
    for e in (2, 1, 3):
        send(code_q, wg_q.at[f, p], 2, w_x.at[0], at_x(e))
    output_x(0)
    for d in NEAR_FIRST:
        factors_x(d)

    own_q.wait()
    own_o.wait()
    query_z(0)
    output_y(0)

    for d in (0,) + NEAR_FIRST:
        arrived(pf.at[pl.ds(0, 3), t], a_x.at[d])
        part = pf.at[pl.ds(rows_at(d), NX), t]
        send(part, part, 1, a_c.at[0], other_core)
    arrived(pf.at[:, 1 - t], a_c.at[0])
    outs = [pltpu.make_async_copy(pf, pf_out, loc.at[0])]
    outs[0].start()

    for c in loads[4:8]:
        c.wait()

    def partial_low(tokens, whole, cot, depth):
        reduced = jnp.dot(
            tokens[...], whole.reshape(depth, RANK), preferred_element_type=jnp.float32
        )
        high = reduced.astype(jnp.bfloat16)
        rest = (reduced - high.astype(jnp.float32)).astype(jnp.bfloat16)
        both = jnp.concatenate([high, rest], axis=0)
        return lax.dot_general(
            both, jnp.concatenate([cot, cot], axis=0),
            (((0,), (0,)), ((), ())), preferred_element_type=jnp.float32,
        )

    def put(par, lo, block):
        for zz in range(NZ):
            for xx in range(NX):
                r = (zz * NX + xx) * 8
                lb[par, xx, zz, :, lo : lo + block.shape[1]] = block[r : r + 8, :]

    low_o = partial_low(x_at, pf[:, :, 32:, :], c_o[...], DA)
    put(0, 512, low_o[:, :256])
    put(1, 0, low_o[:, 256:])
    put(0, 0, partial_low(x_in, pf[:, :, :32, :], c_q[...], D))

    chunks = (
        (2, 0, 8, 1), (3, 0, 8, NY - 1), (1, 0, 4, 1), (1, 4, 4, NY - 1), (0, 0, 4, 1), (0, 4, 4, NY - 1),
    )
    for n, (e, lo, rows, step) in enumerate(chunks):
        part = (x + e) % NX, pl.ds(lo, rows)
        cb[part] = coded(lb[(o,) + part])
        send(cb.at[part], by.at[part], 6, b_y.at[n], at_y(step))
    query_z(1)
    for d in (1, 7, 2):
        output_x(d)

    for n, (e, lo, rows, step) in enumerate(chunks):
        j = (x + e) % NX
        part = j, pl.ds(lo, rows)
        arrived(by.at[part], b_y.at[n])
        lb[(p,) + part] = lb[(p,) + part] + decoded(by[part])
        if e and lo + rows == NZ:
            cb[NX + e - 1] = coded(lb[p, j])
            send(cb.at[NX + e - 1], bx.at[e - 1], 7, b_x.at[0], at_x(e))
    query_z(2)
    for d in (6, 3, 5, 4):
        output_x(d)
    arrived(bx, b_x.at[0])
    mine = (lb[p, x] + decoded(bx[0])) + (decoded(bx[1]) + decoded(bx[2]))
    lb[o, 0] = mine
    sz[...] = coded(mine)
    for d in (4, 3, 5, 2, 6, 1, 7):
        send(sz.at[(z + d) % NZ], bz.at[d - 1], 8, b_z.at[0], at_z(d))
    query_z(3)
    arrived(bz, b_z.at[0])
    mine = lb[o, 0, z]
    for d in range(7):
        mine = mine + decoded(bz[d])
    ty[...] = mine
    send(ty, by2, 9, b_2.at[0], at_y(2))
    for d in (1, 7, 2):
        output_y(d)
    for c in loads[8:14]:
        c.wait()
    arrived(by2, b_2.at[0])

    low_sum = mine + by2[...]
    low[p] = low_sum
    _, _, normed = moment_update(low_sum, fst[p], snd[p])
    half[f, :, pl.ds(pl.multiple_of(p * HALF, 256), HALF)] = normed.astype(jnp.bfloat16)
    square = normed * normed
    total = square[:, 0:128]
    for k in range(1, 6):
        total = total + square[:, k * 128 : (k + 1) * 128]
    qz[z * 2 + t] = jnp.sum(total, axis=0, keepdims=True)

    def piece(g, n, par):
        return half.at[pl.ds(g, n), :, pl.ds(pl.multiple_of(par * HALF, 256), HALF)]

    for d in NEAR_FIRST:
        send(piece(f, 1, p), piece(f, 1, p), 11, e_z.at[d], at_z(d))
    for d in range(NZ):
        for core, dev in ((0, at_z(d)), (1, at_zt(d) if d else other_core)):
            if d or core:
                row = qz.at[z * 2 + t]
                send(row, row, 13, q_z.at[0], dev)
    send(low.at[p], low.at[p], 10, b_l.at[0], at_y(1))
    query_z(4)
    for d in (6, 3, 5, 4):
        output_y(d)
    for d in (0,) + NEAR_FIRST:
        g = ((z + NZ - d) % NZ) * NX + x
        if d:
            arrived(piece(g, 1, p), e_z.at[d])
        for e in (2, 1, 3):
            send(piece(g, 1, p), piece(g, 1, p), 11, e_x.at[d], at_x(e))
    arrived(qz.at[pl.ds(0, 2 * NZ - 1)], q_z.at[0])
    total = qz[0]
    for k in range(1, 2 * NZ):
        total = total + qz[k]
    qx[x] = total
    for e in (2, 1, 3):
        send(qx.at[x], qx.at[x], 14, q_x.at[0], at_x(e))
    for d in (0,) + NEAR_FIRST:
        row = rows_at(d)
        arrived(piece(0, 3, p), e_x.at[d])
        for side in range(2):
            two = piece(row + 2 * side, 2, p)
            send(two, two, 12, e_y.at[0], at_y(1 if side == 0 else NY - 1))
    arrived(qx.at[pl.ds(0, 3)], q_x.at[0])
    qy[p] = (qx[0] + qx[1]) + (qx[2] + qx[3])
    send(qy.at[p], qy.at[p], 15, q_y.at[0], at_y(1))
    arrived(low.at[o], b_l.at[0])
    arrived(piece(0, 32, o), e_y.at[0])
    arrived(qy.at[o], q_y.at[0])
    qt[...] = qy[0] + qy[1]
    outs += [
        pltpu.make_async_copy(half, half_out, loc.at[2]),
        pltpu.make_async_copy(low, low_out, loc.at[3]),
        pltpu.make_async_copy(qt, total_out, loc.at[4]),
    ]
    for c in outs[1:]:
        c.start()
    arrived(wg_q.at[:, o], w_y.at[0])
    arrived(wg_o.at[:, o], w_y.at[1])
    for c in outs:
        c.wait()
    for kind, ref in enumerate((
        pf.at[pl.ds(0, 31), 0], pf.at[:, 0],
        wg_q.at[pl.ds(0, 31), 0], wg_q.at[:, 0], wg_o.at[pl.ds(0, 31), 0], wg_o.at[:, 0],
        by, bx, bz, by2, low.at[0], piece(0, 31, 0), piece(0, 32, 0),
        qz.at[pl.ds(0, 2 * NZ - 1)], qx.at[pl.ds(0, 3)], qy.at[0],
    )):
        remote(ref, ref, sent.at[kind], sent.at[kind], other_core).wait_send()


def gathered(inputs, query_cot, attended, output_cot, proj_q, proj_o, w_q, w_o,
             first_q, second_q, first_o, second_o):
    f32, bf16 = jnp.float32, jnp.bfloat16
    anywhere = pl.BlockSpec(memory_space=pl.ANY)
    dma = pltpu.SemaphoreType.DMA
    shared = (
        ((32, 2, 48, RANK), bf16),
        ((32, 8, 2 * HALF), bf16),
        ((2, 8, HALF), f32),
    )
    return pl.pallas_call(
        comm_kernel,
        out_shape=tuple(jax.ShapeDtypeStruct(*s) for s in shared) + (
            jax.ShapeDtypeStruct((1, 128), f32),
            jax.ShapeDtypeStruct((32, 2, 32, 512), bf16),
            jax.ShapeDtypeStruct((32, 2, 16, 1024), bf16),
        ),
        in_specs=[anywhere] * 12,
        out_specs=(anywhere,) * 6,
        scratch_shapes=[pltpu.VMEM(*s) for s in shared] + [
            pltpu.VMEM((128, D), bf16),
            pltpu.VMEM((128, 512), bf16),
            pltpu.VMEM((128, DA), bf16),
            pltpu.VMEM((128, 1024), bf16),
            pltpu.VMEM((2, 8, HALF), f32),
            pltpu.VMEM((2, 8, HALF), f32),
            pltpu.VMEM((32, 512), f32),
            pltpu.VMEM((16, 1024), f32),
            pltpu.VMEM((32, 512), bf16),
            pltpu.VMEM((16, 1024), bf16),
            pltpu.VMEM((2, NX, NZ, 8, HALF), f32),
            pltpu.VMEM((7, NZ, 8, HALF), bf16),
            pltpu.VMEM((NX, NZ, 8, HALF), bf16),
            pltpu.VMEM((3, NZ, 8, HALF), bf16),
            pltpu.VMEM((NZ, 8, HALF), bf16),
            pltpu.VMEM((7, 8, HALF), bf16),
            pltpu.VMEM((8, HALF), f32),
            pltpu.VMEM((8, HALF), f32),
            pltpu.VMEM((2 * NZ, 1, 128), f32),
            pltpu.VMEM((NX, 1, 128), f32),
            pltpu.VMEM((2, 1, 128), f32),
            pltpu.VMEM((1, 128), f32),
            dma((14,)), dma((16,)), dma((8,)), dma((8,)), dma((1,)), dma((9,)), dma((5, 2)), dma((8,)), dma((2,)),
            dma((6,)), dma((1,)), dma((1,)), dma((1,)), dma((1,)),
            dma((8,)), dma((8,)), dma((1,)), dma((1,)), dma((1,)), dma((1,)),
        ],
        compiler_params=pltpu.CompilerParams(collective_id=0, has_side_effects=True),
    )(
        inputs, query_cot, attended, output_cot,
        proj_q.reshape(2, 32, RANK), proj_o.reshape(2, 16, RANK),
        w_q.reshape(2, 32, 512), w_o.reshape(2, 16, 1024),
        first_q, second_q, first_o, second_o,
    )


def final_kernel(
    pf, wq, wo, half, low, total, proj_q, proj_o, weight_q, weight_o,
    first_q, second_q, first_o, second_o,
    new_q, new_o, step_q, step_o, nf_q, ns_q, nf_o, ns_o, copy_q, copy_o,
):
    mean = jnp.sum(total[...], axis=1, keepdims=True) / (RANK * (DA + D))
    scale = lax.rsqrt(mean + mean_eps)

    def step(factor, lo, width):
        rows = half[:, :, lo : lo + width].reshape(RANK, width)
        return scale * jnp.dot(factor, rows, preferred_element_type=jnp.float32)

    rows_q, rows_o = copy_q.shape[0], copy_o.shape[0]
    all_q = step(pf[:, :, :32, :].reshape(rows_q, RANK), 0, 512)
    copy_q[...] = (decoded(wq[...].reshape(rows_q, 512)) - learn_rate * all_q).astype(jnp.bfloat16)
    all_o = step(pf[:, :, 32:, :].reshape(rows_o, RANK), 512, 1024)
    copy_o[...] = (decoded(wo[...].reshape(rows_o, 1024)) - learn_rate * all_o).astype(jnp.bfloat16)

    @pl.when(pl.program_id(0) == 0)
    def _():
        mine_q = step(proj_q[...], 0, 512)
        step_q[...] = mine_q
        new_q[...] = weight_q[...] - learn_rate * mine_q
        mine_o = step(proj_o[...], 512, 1024)
        step_o[...] = mine_o
        new_o[...] = weight_o[...] - learn_rate * mine_o
        nf_q[...], ns_q[...], _ = moment_update(low[0, :, :512], first_q[...], second_q[...])
        nf_o[:, :256], ns_o[:, :256], _ = moment_update(
            low[0, :, 512:], first_o[:, :256], second_o[:, :256]
        )
        nf_o[:, 256:], ns_o[:, 256:], _ = moment_update(low[1], first_o[:, 256:], second_o[:, 256:])


STEPS = 8


def finished(pf, wq, wo, half, low, total, proj_q, proj_o, weight_q, weight_o,
             first_q, second_q, first_o, second_o):
    f32, bf16 = jnp.float32, jnp.bfloat16

    def blocks(shape):
        rest = (0,) * (len(shape) - 1)
        return pl.BlockSpec((shape[0] // STEPS,) + tuple(shape[1:]), lambda i: (i,) + rest)

    def whole(shape):
        return pl.BlockSpec(tuple(shape), lambda i: (0,) * len(shape))

    small = (half, low, total, proj_q, proj_o, weight_q, weight_o, first_q, second_q, first_o, second_o)
    outs = (
        ((64, 512), f32), ((32, 1024), f32), ((64, 512), f32), ((32, 1024), f32),
        ((8, 512), f32), ((8, 512), f32), ((8, 1024), f32), ((8, 1024), f32),
        ((D, 512), bf16), ((DA, 1024), bf16),
    )
    return pl.pallas_call(
        final_kernel,
        grid=(STEPS,),
        out_shape=tuple(jax.ShapeDtypeStruct(*s) for s in outs),
        in_specs=[blocks(a.shape) for a in (pf, wq, wo)] + [whole(a.shape) for a in small],
        out_specs=tuple(whole(s) for s, _ in outs[:8]) + tuple(blocks(s) for s, _ in outs[8:]),
        cost_estimate=pl.CostEstimate(flops=2_200_000_000, bytes_accessed=12_000_000, transcendentals=0),
    )(pf, wq, wo, *small)


def local(
    inputs, query_cot, attended, output_cot, proj_query, proj_output,
    weight_query, weight_output, first_query, second_query, first_output, second_output,
):
    pf, half, low, total, wg_q, wg_o = gathered(
        inputs, query_cot, attended, output_cot, proj_query, proj_output,
        weight_query, weight_output, first_query, second_query, first_output, second_output,
    )
    return finished(
        pf, wg_q, wg_o, half, low, total, proj_query, proj_output, weight_query, weight_output,
        first_query, second_query, first_output, second_output,
    )


def solution(mesh):
    return jax.shard_map(
        local,
        mesh=mesh,
        in_specs=(
            P(("fs", "rep"), None),
            P(("fs", "rep"), "tp"),
            P(("fs", "rep"), None),
            P(("fs", "rep"), "tp"),
            P("fs", None),
            P("fs", None),
            P("fs", "tp"),
            P("fs", "tp"),
            P("fs", "tp"),
            P("fs", "tp"),
            P("fs", "tp"),
            P("fs", "tp"),
        ),
        out_specs=(
            P("fs", "tp"),
            P("fs", "tp"),
            P("fs", "tp"),
            P("fs", "tp"),
            P("fs", "tp"),
            P("fs", "tp"),
            P("fs", "tp"),
            P("fs", "tp"),
            P(None, "tp"),
            P(None, "tp"),
        ),
        check_vma=False,
    )
```

time: 83.3 us -> 73 us (0.88)
  Pallas kernels: 82.4 us -> 72.1 us
    pallas_call x1, Pallas kernels: 72.9 us -> 62.6 us  [gathered(): pl.pallas_call(comm_kernel, out_shape=tuple((jax.ShapeDtypeStruct(*s) for...]
where the time goes in v3:
time: 73 us; the launch traced here: 72.7 us
  Pallas kernels  72.1 us (99%)
    pallas_call x1, Pallas kernels, gathered(): pl.pallas_call(comm_kernel, out_shape=tuple((jax.ShapeDtypeStruct(*s) for...  62.6 us
    pallas_call x1, Pallas kernels, finished(): pl.pallas_call(final_kernel, grid=(STEPS,), out_shape=tuple((jax.ShapeDty...  9.49 us

profile of v3, /device:TPU:1, one launch (start us, length us, event | category | flops | bytes accessed | tf_op | source)
XLA Modules:
  0.0 72.7 jit_solution(5553624981582864339)
XLA Ops:
  0.6 62.6 %shard_map.195 = (bf16[32,2,48,256]{3,2,1,0:T(8,128)(2,1)}, bf16[32,8,1536]{2,1,0:T(8,128)(2,1)}, f32[2,8,768]{2,1,0:T(8,128)}, f32[1,128]{1,0:T(1,128)}, bf16[3...) custom-call(bf16[128,2048]{1,0:T(8,128)(2,1)} %inputs.1, bf16[128,512]{1,0:T(8,128)(2,1)} %query_cot.1, ...), custom_call_target="tpu_custom_call" | custom-call | tf_op jit(solution)/shard_map/pallas_call | solution.py:346
  63.2 9.5 %shard_map.196 = (f32[64,512]{1,0:T(8,128)}, f32[32,1024]{1,0:T(8,128)}, f32[64,512]{1,0:T(8,128)}, f32[32,1024]{1,0:T(8,128)}, f32[8,512]{1,0:T(8,128)}, /*inde...) custom-call(bf16[32,2,48,256]{3,2,1,0:T(8,128)(2,1)} %get-tuple-elem, ...), custom_call_target="tpu_custom_call" | custom-call | flops 2200000000 | bytes 12000000 | tf_op jit(solution)/shard_map/pallas_call | solution.py:444

commit v4 on v3

--- a/solution.py
+++ b/solution.py
@@ -244,6 +244,8 @@
     query_z(2)
     for d in (6, 3, 5, 4):
         output_x(d)
+    for d in (1, 7, 2):
+        output_y(d)
     arrived(bx, b_x.at[0])
     mine = (lb[p, x] + decoded(bx[0])) + (decoded(bx[1]) + decoded(bx[2]))
     lb[o, 0] = mine
@@ -257,7 +259,8 @@
         mine = mine + decoded(bz[d])
     ty[...] = mine
     send(ty, by2, 9, b_2.at[0], at_y(2))
-    for d in (1, 7, 2):
+    query_z(4)
+    for d in (6, 3, 5, 4):
         output_y(d)
     for c in loads[8:14]:
         c.wait()
@@ -284,9 +287,6 @@
                 row = qz.at[z * 2 + t]
                 send(row, row, 13, q_z.at[0], dev)
     send(low.at[p], low.at[p], 10, b_l.at[0], at_y(1))
-    query_z(4)
-    for d in (6, 3, 5, 4):
-        output_y(d)
     for d in (0,) + NEAR_FIRST:
         g = ((z + NZ - d) % NZ) * NX + x
         if d:
@@ -421,7 +421,7 @@
         nf_o[:, 256:], ns_o[:, 256:], _ = moment_update(low[1], first_o[:, 256:], second_o[:, 256:])
 
 
-STEPS = 8
+STEPS = 4
 
 
 def finished(pf, wq, wo, half, low, total, proj_q, proj_o, weight_q, weight_o,

time: 73 us -> 69.2 us (0.948)
  Pallas kernels: 72.1 us -> 68.3 us
    pallas_call x1, Pallas kernels: 62.6 us -> 60.3 us  [gathered(): pl.pallas_call(comm_kernel, out_shape=tuple((jax.ShapeDtypeStruct(*s) for...]
    pallas_call x1, Pallas kernels: 9.49 us -> 7.93 us  [finished(): pl.pallas_call(final_kernel, grid=(STEPS,), out_shape=tuple((jax.ShapeDty...]
where the time goes in v4:
time: 69.2 us; the launch traced here: 68.9 us
  Pallas kernels  68.3 us (99%)
    pallas_call x1, Pallas kernels, gathered(): pl.pallas_call(comm_kernel, out_shape=tuple((jax.ShapeDtypeStruct(*s) for...  60.3 us
    pallas_call x1, Pallas kernels, finished(): pl.pallas_call(final_kernel, grid=(STEPS,), out_shape=tuple((jax.ShapeDty...  7.93 us

profile of v4, /device:TPU:1, one launch (start us, length us, event | category | flops | bytes accessed | tf_op | source)
XLA Modules:
  0.0 68.9 jit_solution(11672594662769264303)
XLA Ops:
  0.6 60.3 %shard_map.195 = (bf16[32,2,48,256]{3,2,1,0:T(8,128)(2,1)}, bf16[32,8,1536]{2,1,0:T(8,128)(2,1)}, f32[2,8,768]{2,1,0:T(8,128)}, f32[1,128]{1,0:T(1,128)}, bf16[3...) custom-call(bf16[128,2048]{1,0:T(8,128)(2,1)} %inputs.1, bf16[128,512]{1,0:T(8,128)(2,1)} %query_cot.1, ...), custom_call_target="tpu_custom_call" | custom-call | tf_op jit(solution)/shard_map/pallas_call | solution.py:346
  61.0 7.9 %shard_map.196 = (f32[64,512]{1,0:T(8,128)}, f32[32,1024]{1,0:T(8,128)}, f32[64,512]{1,0:T(8,128)}, f32[32,1024]{1,0:T(8,128)}, f32[8,512]{1,0:T(8,128)}, /*inde...) custom-call(bf16[32,2,48,256]{3,2,1,0:T(8,128)(2,1)} %get-tuple-elem, ...), custom_call_target="tpu_custom_call" | custom-call | flops 2200000000 | bytes 12000000 | tf_op jit(solution)/shard_map/pallas_call | solution.py:444

commit v5 on v4

--- a/solution.py
+++ b/solution.py
@@ -48,7 +48,7 @@
     pf_out, half_out, low_out, total_out, wg_q, wg_o,
     pf, half, low,
     x_in, c_q, x_at, c_o, fst, snd, old_q, old_o, code_q, code_o,
-    lb, cb, by, bx, sz, bz, ty, by2, qz, qx, qy, qt,
+    lb_o, lb_q, cb_o, cb_q, by_o, by_q, bx_o, bx_q, sz, bz, ty, by2, qz, qx, qy, qt,
     loc, sent, a_z, a_x, a_c, w_x, w_z, w_d, w_y, b_y, b_x, b_z, b_2, b_l,
     e_z, e_x, e_y, q_z, q_x, q_y,
 ):
@@ -95,12 +95,14 @@
         pltpu.make_async_copy(attended, x_at, loc.at[3]),
         pltpu.make_async_copy(query_cot, c_q, loc.at[4]),
         pltpu.make_async_copy(output_cot, c_o, loc.at[5]),
-        pltpu.make_async_copy(first_q, fst.at[0, :, pl.ds(0, 512)], loc.at[6]),
-        pltpu.make_async_copy(first_o.at[:, pl.ds(0, 256)], fst.at[0, :, pl.ds(512, 256)], loc.at[7]),
-        pltpu.make_async_copy(first_o.at[:, pl.ds(256, 768)], fst.at[1], loc.at[8]),
-        pltpu.make_async_copy(second_q, snd.at[0, :, pl.ds(0, 512)], loc.at[9]),
-        pltpu.make_async_copy(second_o.at[:, pl.ds(0, 256)], snd.at[0, :, pl.ds(512, 256)], loc.at[10]),
-        pltpu.make_async_copy(second_o.at[:, pl.ds(256, 768)], snd.at[1], loc.at[11]),
+        pltpu.make_async_copy(first_o.at[:, pl.ds(0, 512)], fst.at[0, :, pl.ds(0, 512)], loc.at[6]),
+        pltpu.make_async_copy(first_o.at[:, pl.ds(512, 512)], fst.at[1, :, pl.ds(0, 512)], loc.at[7]),
+        pltpu.make_async_copy(first_q.at[:, pl.ds(0, 256)], fst.at[0, :, pl.ds(512, 256)], loc.at[8]),
+        pltpu.make_async_copy(first_q.at[:, pl.ds(256, 256)], fst.at[1, :, pl.ds(512, 256)], loc.at[9]),
+        pltpu.make_async_copy(second_o.at[:, pl.ds(0, 512)], snd.at[0, :, pl.ds(0, 512)], loc.at[10]),
+        pltpu.make_async_copy(second_o.at[:, pl.ds(512, 512)], snd.at[1, :, pl.ds(0, 512)], loc.at[11]),
+        pltpu.make_async_copy(second_q.at[:, pl.ds(0, 256)], snd.at[0, :, pl.ds(512, 256)], loc.at[14]),
+        pltpu.make_async_copy(second_q.at[:, pl.ds(256, 256)], snd.at[1, :, pl.ds(512, 256)], loc.at[15]),
     ]
     for c in loads:
         c.start()
@@ -121,15 +123,18 @@
     own_o.start()
     pl.semaphore_wait(barrier, len(peers))
 
-    for d in NEAR_FIRST:
-        send(pf.at[f, t], pf.at[f, t], 0, a_z.at[d], at_z(d))
-
-    def factors_x(d):
-        g = ((z + NZ - d) % NZ) * NX + x
+    factor_rows = (pl.ds(32, 16), pl.ds(0, 32))
+    for k, rows in enumerate(factor_rows):
+        for d in NEAR_FIRST:
+            own = pf.at[f, t, rows]
+            send(own, own, 0, a_z.at[k, d], at_z(d))
+
+    def factors_x(k, d):
+        part = pf.at[((z + NZ - d) % NZ) * NX + x, t, factor_rows[k]]
         if d:
-            arrived(pf.at[g, t], a_z.at[d])
+            arrived(part, a_z.at[k, d])
         for e in (2, 1, 3):
-            send(pf.at[g, t], pf.at[g, t], 0, a_x.at[d], at_x(e))
+            send(part, part, 0, a_x.at[k, d], at_x(e))
 
     def rows_at(d):
         return ((z + NZ - d) % NZ) * NX
@@ -158,12 +163,10 @@
             part = wg_q.at[pl.ds(rows_at(0), NX), p]
             send(part, part, 2, w_z.at[1, 0], at_z(1))
             send(part, part, 2, w_z.at[1, 1], at_z(NZ - 1))
-            weights_y(0, 0)
             return
         if s == NZ // 2:
             for way in range(2):
                 arrived(wg_q.at[pl.ds(rows_at(s) + 2 * way, 2), p], w_z.at[s, way])
-            weights_y(0, s)
             return
         for way, sign in ((0, 1), (1, -1)):
             part = wg_q.at[pl.ds(rows_at(sign * s), NX), p]
@@ -171,33 +174,35 @@
             if s == NZ // 2 - 1:
                 part = wg_q.at[pl.ds(rows_at(sign * s) + 2 * way, 2), p]
             send(part, part, 2, w_z.at[s + 1, way], at_z(sign % NZ))
-        for sign in (1, -1):
-            weights_y(0, sign * s)
+
+    def query_y(s):
+        for d in ((s, NZ - s) if s % (NZ // 2) else (s,)):
+            weights_y(0, d)
 
     for d in NEAR_FIRST:
         send(code_o, wg_o.at[f, p], 4, w_d.at[d], at_z(d))
-    factors_x(0)
+    factors_x(0, 0)
+    factors_x(1, 0)
     for e in (2, 1, 3):
         send(code_q, wg_q.at[f, p], 2, w_x.at[0], at_x(e))
     output_x(0)
-    for d in NEAR_FIRST:
-        factors_x(d)
+    for k in range(2):
+        for d in NEAR_FIRST:
+            factors_x(k, d)
 
     own_q.wait()
     own_o.wait()
     query_z(0)
+    query_y(0)
     output_y(0)
 
-    for d in (0,) + NEAR_FIRST:
-        arrived(pf.at[pl.ds(0, 3), t], a_x.at[d])
-        part = pf.at[pl.ds(rows_at(d), NX), t]
-        send(part, part, 1, a_c.at[0], other_core)
-    arrived(pf.at[:, 1 - t], a_c.at[0])
-    outs = [pltpu.make_async_copy(pf, pf_out, loc.at[0])]
-    outs[0].start()
-
-    for c in loads[4:8]:
-        c.wait()
+    def factors_core(k):
+        rows = factor_rows[k]
+        for d in (0,) + NEAR_FIRST:
+            arrived(pf.at[pl.ds(0, 3), t, rows], a_x.at[k, d])
+            part = pf.at[pl.ds(rows_at(d), NX), t, rows]
+            send(part, part, 1, a_c.at[k], other_core)
+        arrived(pf.at[:, 1 - t, rows], a_c.at[k])
 
     def partial_low(tokens, whole, cot, depth):
         reduced = jnp.dot(
@@ -211,65 +216,86 @@
             (((0,), (0,)), ((), ())), preferred_element_type=jnp.float32,
         )
 
-    def put(par, lo, block):
-        for zz in range(NZ):
-            for xx in range(NX):
-                r = (zz * NX + xx) * 8
-                lb[par, xx, zz, :, lo : lo + block.shape[1]] = block[r : r + 8, :]
-
-    low_o = partial_low(x_at, pf[:, :, 32:, :], c_o[...], DA)
-    put(0, 512, low_o[:, :256])
-    put(1, 0, low_o[:, 256:])
-    put(0, 0, partial_low(x_in, pf[:, :, :32, :], c_q[...], D))
+    def put(lb, block):
+        width = block.shape[1] // 2
+        for par in range(2):
+            for zz in range(NZ):
+                for xx in range(NX):
+                    r = (zz * NX + xx) * 8
+                    lb[par, xx, zz] = block[r : r + 8, par * width : (par + 1) * width]
 
     chunks = (
         (2, 0, 8, 1), (3, 0, 8, NY - 1), (1, 0, 4, 1), (1, 4, 4, NY - 1), (0, 0, 4, 1), (0, 4, 4, NY - 1),
     )
-    for n, (e, lo, rows, step) in enumerate(chunks):
-        part = (x + e) % NX, pl.ds(lo, rows)
-        cb[part] = coded(lb[(o,) + part])
-        send(cb.at[part], by.at[part], 6, b_y.at[n], at_y(step))
+
+    def sums_y(k, lb, cb, by):
+        for n, (e, lo, rows, step) in enumerate(chunks):
+            part = (x + e) % NX, pl.ds(lo, rows)
+            cb[part] = coded(lb[(o,) + part])
+            send(cb.at[part], by.at[part], 6 + k, b_y.at[k, n], at_y(step))
+
+    def sums_x(k, lb, cb, by, bx):
+        for n, (e, lo, rows, step) in enumerate(chunks):
+            j = (x + e) % NX
+            part = j, pl.ds(lo, rows)
+            arrived(by.at[part], b_y.at[k, n])
+            lb[(p,) + part] = lb[(p,) + part] + decoded(by[part])
+            if e and lo + rows == NZ:
+                cb[NX + e - 1] = coded(lb[p, j])
+                send(cb.at[NX + e - 1], bx.at[e - 1], 16 + k, b_x.at[k], at_x(e))
+
+    factors_core(0)
+    loads[5].wait()
+    loads[7].wait()
+    put(lb_o, partial_low(x_at, pf[:, :, 32:, :], c_o[...], DA))
+    sums_y(0, lb_o, cb_o, by_o)
+    output_x(1)
+    output_x(7)
+    factors_core(1)
     query_z(1)
-    for d in (1, 7, 2):
+    outs = [pltpu.make_async_copy(pf, pf_out, loc.at[0])]
+    outs[0].start()
+    loads[4].wait()
+    loads[6].wait()
+    put(lb_q, partial_low(x_in, pf[:, :, :32, :], c_q[...], D))
+    sums_y(1, lb_q, cb_q, by_q)
+    query_y(1)
+
+    sums_x(0, lb_o, cb_o, by_o, bx_o)
+    sums_x(1, lb_q, cb_q, by_q, bx_q)
+    for d in (2, 6, 3, 5, 4):
         output_x(d)
-
-    for n, (e, lo, rows, step) in enumerate(chunks):
-        j = (x + e) % NX
-        part = j, pl.ds(lo, rows)
-        arrived(by.at[part], b_y.at[n])
-        lb[(p,) + part] = lb[(p,) + part] + decoded(by[part])
-        if e and lo + rows == NZ:
-            cb[NX + e - 1] = coded(lb[p, j])
-            send(cb.at[NX + e - 1], bx.at[e - 1], 7, b_x.at[0], at_x(e))
+    output_y(1)
+    output_y(7)
     query_z(2)
-    for d in (6, 3, 5, 4):
-        output_x(d)
-    for d in (1, 7, 2):
-        output_y(d)
-    arrived(bx, b_x.at[0])
-    mine = (lb[p, x] + decoded(bx[0])) + (decoded(bx[1]) + decoded(bx[2]))
-    lb[o, 0] = mine
-    sz[...] = coded(mine)
+    query_y(2)
+    for k, (lb, bx) in enumerate(((lb_o, bx_o), (lb_q, bx_q))):
+        arrived(bx, b_x.at[k])
+        part = (lb[p, x] + decoded(bx[0])) + (decoded(bx[1]) + decoded(bx[2]))
+        lb[o, 0] = part
+        sz[:, :, pl.ds(512 * k, part.shape[2])] = coded(part)
     for d in (4, 3, 5, 2, 6, 1, 7):
         send(sz.at[(z + d) % NZ], bz.at[d - 1], 8, b_z.at[0], at_z(d))
+    output_y(2)
     query_z(3)
     arrived(bz, b_z.at[0])
-    mine = lb[o, 0, z]
+    mine = jnp.concatenate([lb_o[o, 0, z], lb_q[o, 0, z]], axis=1)
     for d in range(7):
         mine = mine + decoded(bz[d])
     ty[...] = mine
     send(ty, by2, 9, b_2.at[0], at_y(2))
+    query_y(3)
+    output_y(6)
+    output_y(3)
     query_z(4)
-    for d in (6, 3, 5, 4):
-        output_y(d)
-    for c in loads[8:14]:
+    for c in loads[8:16]:
         c.wait()
     arrived(by2, b_2.at[0])
 
     low_sum = mine + by2[...]
     low[p] = low_sum
     _, _, normed = moment_update(low_sum, fst[p], snd[p])
-    half[f, :, pl.ds(pl.multiple_of(p * HALF, 256), HALF)] = normed.astype(jnp.bfloat16)
+    half[p, f] = normed.astype(jnp.bfloat16)
     square = normed * normed
     total = square[:, 0:128]
     for k in range(1, 6):
@@ -277,7 +303,7 @@
     qz[z * 2 + t] = jnp.sum(total, axis=0, keepdims=True)
 
     def piece(g, n, par):
-        return half.at[pl.ds(g, n), :, pl.ds(pl.multiple_of(par * HALF, 256), HALF)]
+        return half.at[par, pl.ds(g, n)]
 
     for d in NEAR_FIRST:
         send(piece(f, 1, p), piece(f, 1, p), 11, e_z.at[d], at_z(d))
@@ -287,6 +313,9 @@
                 row = qz.at[z * 2 + t]
                 send(row, row, 13, q_z.at[0], dev)
     send(low.at[p], low.at[p], 10, b_l.at[0], at_y(1))
+    query_y(4)
+    output_y(5)
+    output_y(4)
     for d in (0,) + NEAR_FIRST:
         g = ((z + NZ - d) % NZ) * NX + x
         if d:
@@ -327,8 +356,9 @@
     for kind, ref in enumerate((
         pf.at[pl.ds(0, 31), 0], pf.at[:, 0],
         wg_q.at[pl.ds(0, 31), 0], wg_q.at[:, 0], wg_o.at[pl.ds(0, 31), 0], wg_o.at[:, 0],
-        by, bx, bz, by2, low.at[0], piece(0, 31, 0), piece(0, 32, 0),
+        by_o, by_q, bz, by2, low.at[0], piece(0, 31, 0), piece(0, 32, 0),
         qz.at[pl.ds(0, 2 * NZ - 1)], qx.at[pl.ds(0, 3)], qy.at[0],
+        bx_o, bx_q,
     )):
         remote(ref, ref, sent.at[kind], sent.at[kind], other_core).wait_send()
 
@@ -340,7 +370,7 @@
     dma = pltpu.SemaphoreType.DMA
     shared = (
         ((32, 2, 48, RANK), bf16),
-        ((32, 8, 2 * HALF), bf16),
+        ((2, 32, 8, HALF), bf16),
         ((2, 8, HALF), f32),
     )
     return pl.pallas_call(
@@ -363,10 +393,14 @@
             pltpu.VMEM((16, 1024), f32),
             pltpu.VMEM((32, 512), bf16),
             pltpu.VMEM((16, 1024), bf16),
-            pltpu.VMEM((2, NX, NZ, 8, HALF), f32),
-            pltpu.VMEM((7, NZ, 8, HALF), bf16),
-            pltpu.VMEM((NX, NZ, 8, HALF), bf16),
-            pltpu.VMEM((3, NZ, 8, HALF), bf16),
+            pltpu.VMEM((2, NX, NZ, 8, 512), f32),
+            pltpu.VMEM((2, NX, NZ, 8, 256), f32),
+            pltpu.VMEM((7, NZ, 8, 512), bf16),
+            pltpu.VMEM((7, NZ, 8, 256), bf16),
+            pltpu.VMEM((NX, NZ, 8, 512), bf16),
+            pltpu.VMEM((NX, NZ, 8, 256), bf16),
+            pltpu.VMEM((3, NZ, 8, 512), bf16),
+            pltpu.VMEM((3, NZ, 8, 256), bf16),
             pltpu.VMEM((NZ, 8, HALF), bf16),
             pltpu.VMEM((7, 8, HALF), bf16),
             pltpu.VMEM((8, HALF), f32),
@@ -375,8 +409,8 @@
             pltpu.VMEM((NX, 1, 128), f32),
             pltpu.VMEM((2, 1, 128), f32),
             pltpu.VMEM((1, 128), f32),
-            dma((14,)), dma((16,)), dma((8,)), dma((8,)), dma((1,)), dma((9,)), dma((5, 2)), dma((8,)), dma((2,)),
-            dma((6,)), dma((1,)), dma((1,)), dma((1,)), dma((1,)),
+            dma((16,)), dma((18,)), dma((2, 8)), dma((2, 8)), dma((2,)), dma((9,)), dma((5, 2)), dma((8,)), dma((2,)),
+            dma((2, 6)), dma((2,)), dma((1,)), dma((1,)), dma((1,)),
             dma((8,)), dma((8,)), dma((1,)), dma((1,)), dma((1,)), dma((1,)),
         ],
         compiler_params=pltpu.CompilerParams(collective_id=0, has_side_effects=True),
@@ -396,29 +430,37 @@
     mean = jnp.sum(total[...], axis=1, keepdims=True) / (RANK * (DA + D))
     scale = lax.rsqrt(mean + mean_eps)
 
-    def step(factor, lo, width):
-        rows = half[:, :, lo : lo + width].reshape(RANK, width)
+    def step(factor, h, lo, width):
+        rows = half[h, :, :, lo : lo + width].reshape(RANK, width)
         return scale * jnp.dot(factor, rows, preferred_element_type=jnp.float32)
 
     rows_q, rows_o = copy_q.shape[0], copy_o.shape[0]
-    all_q = step(pf[:, :, :32, :].reshape(rows_q, RANK), 0, 512)
-    copy_q[...] = (decoded(wq[...].reshape(rows_q, 512)) - learn_rate * all_q).astype(jnp.bfloat16)
-    all_o = step(pf[:, :, 32:, :].reshape(rows_o, RANK), 512, 1024)
-    copy_o[...] = (decoded(wo[...].reshape(rows_o, 1024)) - learn_rate * all_o).astype(jnp.bfloat16)
-
-    @pl.when(pl.program_id(0) == 0)
+    own = pl.program_id(0) == 0
+    for h in range(2):
+        at_o, at_q = pl.ds(512 * h, 512), pl.ds(256 * h, 256)
+        all_o = step(pf[:, :, 32:, :].reshape(rows_o, RANK), h, 0, 512)
+        old_o = decoded(wo[:, :, :, at_o].reshape(rows_o, 512))
+        copy_o[:, at_o] = (old_o - learn_rate * all_o).astype(jnp.bfloat16)
+        all_q = step(pf[:, :, :32, :].reshape(rows_q, RANK), h, 512, 256)
+        old_q = decoded(wq[:, :, :, at_q].reshape(rows_q, 256))
+        copy_q[:, at_q] = (old_q - learn_rate * all_q).astype(jnp.bfloat16)
+
+    @pl.when(own)
     def _():
-        mine_q = step(proj_q[...], 0, 512)
-        step_q[...] = mine_q
-        new_q[...] = weight_q[...] - learn_rate * mine_q
-        mine_o = step(proj_o[...], 512, 1024)
-        step_o[...] = mine_o
-        new_o[...] = weight_o[...] - learn_rate * mine_o
-        nf_q[...], ns_q[...], _ = moment_update(low[0, :, :512], first_q[...], second_q[...])
-        nf_o[:, :256], ns_o[:, :256], _ = moment_update(
-            low[0, :, 512:], first_o[:, :256], second_o[:, :256]
-        )
-        nf_o[:, 256:], ns_o[:, 256:], _ = moment_update(low[1], first_o[:, 256:], second_o[:, 256:])
+        for h in range(2):
+            at_o, at_q = pl.ds(512 * h, 512), pl.ds(256 * h, 256)
+            mine_o = step(proj_o[...], h, 0, 512)
+            step_o[:, at_o] = mine_o
+            new_o[:, at_o] = weight_o[:, at_o] - learn_rate * mine_o
+            mine_q = step(proj_q[...], h, 512, 256)
+            step_q[:, at_q] = mine_q
+            new_q[:, at_q] = weight_q[:, at_q] - learn_rate * mine_q
+            nf_o[:, at_o], ns_o[:, at_o], _ = moment_update(
+                low[h, :, :512], first_o[:, at_o], second_o[:, at_o]
+            )
+            nf_q[:, at_q], ns_q[:, at_q], _ = moment_update(
+                low[h, :, 512:], first_q[:, at_q], second_q[:, at_q]
+            )
 
 
 STEPS = 4

time: 69.2 us -> 66 us (0.954)
  Pallas kernels: 68.3 us -> 65.2 us
    pallas_call x1, Pallas kernels: 60.3 us -> 57.2 us  [gathered(): pl.pallas_call(comm_kernel, out_shape=tuple((jax.ShapeDtypeStruct(*s) for...]
where the time goes in v5:
time: 66 us; the launch traced here: 65.8 us
  Pallas kernels  65.2 us (99%)
    pallas_call x1, Pallas kernels, gathered(): pl.pallas_call(comm_kernel, out_shape=tuple((jax.ShapeDtypeStruct(*s) for...  57.2 us
    pallas_call x1, Pallas kernels, finished(): pl.pallas_call(final_kernel, grid=(STEPS,), out_shape=tuple((jax.ShapeDty...  7.97 us

profile of v5, /device:TPU:1, one launch (start us, length us, event | category | flops | bytes accessed | tf_op | source)
XLA Modules:
  0.0 65.8 jit_solution(2996515201857829529)
XLA Ops:
  0.6 57.2 %shard_map.195 = (bf16[32,2,48,256]{3,2,1,0:T(8,128)(2,1)}, bf16[2,32,8,768]{3,2,1,0:T(8,128)(2,1)}, f32[2,8,768]{2,1,0:T(8,128)}, f32[1,128]{1,0:T(1,128)}, bf1...) custom-call(bf16[128,2048]{1,0:T(8,128)(2,1)} %inputs.1, bf16[128,512]{1,0:T(8,128)(2,1)} %query_cot.1, ...), custom_call_target="tpu_custom_call" | custom-call | tf_op jit(solution)/shard_map/pallas_call | solution.py:376
  57.9 8.0 %shard_map.196 = (f32[64,512]{1,0:T(8,128)}, f32[32,1024]{1,0:T(8,128)}, f32[64,512]{1,0:T(8,128)}, f32[32,1024]{1,0:T(8,128)}, f32[8,512]{1,0:T(8,128)}, /*inde...) custom-call(bf16[32,2,48,256]{3,2,1,0:T(8,128)(2,1)} %get-tuple-elem, ...), custom_call_target="tpu_custom_call" | custom-call | flops 2200000000 | bytes 12000000 | tf_op jit(solution)/shard_map/pallas_call | solution.py:486

commit v6 on v5

--- a/solution.py
+++ b/solution.py
@@ -185,7 +185,6 @@
     factors_x(1, 0)
     for e in (2, 1, 3):
         send(code_q, wg_q.at[f, p], 2, w_x.at[0], at_x(e))
-    output_x(0)
     for k in range(2):
         for d in NEAR_FIRST:
             factors_x(k, d)
@@ -194,7 +193,6 @@
     own_o.wait()
     query_z(0)
     query_y(0)
-    output_y(0)
 
     def factors_core(k):
         rows = factor_rows[k]
@@ -249,17 +247,19 @@
     loads[7].wait()
     put(lb_o, partial_low(x_at, pf[:, :, 32:, :], c_o[...], DA))
     sums_y(0, lb_o, cb_o, by_o)
+    output_x(0)
     output_x(1)
     output_x(7)
     factors_core(1)
-    query_z(1)
     outs = [pltpu.make_async_copy(pf, pf_out, loc.at[0])]
     outs[0].start()
     loads[4].wait()
     loads[6].wait()
     put(lb_q, partial_low(x_in, pf[:, :, :32, :], c_q[...], D))
     sums_y(1, lb_q, cb_q, by_q)
+    query_z(1)
     query_y(1)
+    output_y(0)
 
     sums_x(0, lb_o, cb_o, by_o, bx_o)
     sums_x(1, lb_q, cb_q, by_q, bx_q)
@@ -422,62 +422,120 @@
     )
 
 
+CHUNKS = 4
+
+
 def final_kernel(
-    pf, wq, wo, half, low, total, proj_q, proj_o, weight_q, weight_o,
-    first_q, second_q, first_o, second_o,
-    new_q, new_o, step_q, step_o, nf_q, ns_q, nf_o, ns_o, copy_q, copy_o,
+    pf_in, wq_in, wo_in, half_in, low_in, total_in, proj_q_in, proj_o_in, weight_q_in, weight_o_in,
+    first_q_in, second_q_in, first_o_in, second_o_in,
+    new_q_out, new_o_out, step_q_out, step_o_out, nf_q_out, ns_q_out, nf_o_out, ns_o_out,
+    copy_q_out, copy_o_out,
+    pf, wq, wo, half, rows, small, new, copy_q, copy_o, chunk_sems, small_sems, new_sems, out_sems,
 ):
+    low, total, proj_q, proj_o, weight_q, weight_o, first_q, second_q, first_o, second_o = small
+    new_q, new_o, step_q, step_o, nf_q, ns_q, nf_o, ns_o = new
+    shards = NZ * NX // CHUNKS
+
+    def chunk_loads(i):
+        part = pl.ds(i * shards, shards)
+        return [
+            pltpu.make_async_copy(src.at[part], dst.at[part], chunk_sems.at[k, i])
+            for k, (src, dst) in enumerate(((pf_in, pf), (wq_in, wq), (wo_in, wo)))
+        ]
+
+    small_loads = [
+        pltpu.make_async_copy(src, dst, small_sems.at[k])
+        for k, (src, dst) in enumerate(zip(
+            (low_in, total_in, proj_q_in, proj_o_in, weight_q_in, weight_o_in,
+             first_q_in, second_q_in, first_o_in, second_o_in), small
+        ))
+    ]
+    half_load = pltpu.make_async_copy(half_in, half, small_sems.at[len(small)])
+    half_load.start()
+    small_loads[1].start()
+    for i in range(CHUNKS):
+        for c in chunk_loads(i):
+            c.start()
+    for k, c in enumerate(small_loads):
+        if k != 1:
+            c.start()
+
+    half_load.wait()
+    small_loads[1].wait()
     mean = jnp.sum(total[...], axis=1, keepdims=True) / (RANK * (DA + D))
     scale = lax.rsqrt(mean + mean_eps)
-
-    def step(factor, h, lo, width):
-        rows = half[h, :, :, lo : lo + width].reshape(RANK, width)
-        return scale * jnp.dot(factor, rows, preferred_element_type=jnp.float32)
-
-    rows_q, rows_o = copy_q.shape[0], copy_o.shape[0]
-    own = pl.program_id(0) == 0
+    rate = learn_rate * scale
+    for h in range(2):
+        rows[:, HALF * h : HALF * (h + 1)] = half[h].reshape(RANK, HALF)
+
+    def product(factor, h, lo, width):
+        start = HALF * h + lo
+        return jnp.dot(factor, rows[:, start : start + width], preferred_element_type=jnp.float32)
+
+    rows_q, rows_o = 64 * shards, 32 * shards
+
+    def out_copies(i):
+        part_q, part_o = pl.ds(i * rows_q, rows_q), pl.ds(i * rows_o, rows_o)
+        return (
+            pltpu.make_async_copy(copy_q.at[part_q], copy_q_out.at[part_q], out_sems.at[0, i]),
+            pltpu.make_async_copy(copy_o.at[part_o], copy_o_out.at[part_o], out_sems.at[1, i]),
+        )
+
+    @pl.loop(0, CHUNKS)
+    def _(i):
+        for c in chunk_loads(i):
+            c.wait()
+        part = pl.ds(i * shards, shards)
+        part_q, part_o = pl.ds(i * rows_q, rows_q), pl.ds(i * rows_o, rows_o)
+        factor_o = pf[part, :, 32:, :].reshape(rows_o, RANK)
+        factor_q = pf[part, :, :32, :].reshape(rows_q, RANK)
+        for h in range(2):
+            at_o, at_q = pl.ds(512 * h, 512), pl.ds(256 * h, 256)
+            old_o = decoded(wo[part, :, :, at_o].reshape(rows_o, 512))
+            copy_o[part_o, at_o] = (old_o - rate * product(factor_o, h, 0, 512)).astype(jnp.bfloat16)
+            old_q = decoded(wq[part, :, :, at_q].reshape(rows_q, 256))
+            copy_q[part_q, at_q] = (old_q - rate * product(factor_q, h, 512, 256)).astype(jnp.bfloat16)
+        for c in out_copies(i):
+            c.start()
+
+    for k, c in enumerate(small_loads):
+        if k != 1:
+            c.wait()
     for h in range(2):
         at_o, at_q = pl.ds(512 * h, 512), pl.ds(256 * h, 256)
-        all_o = step(pf[:, :, 32:, :].reshape(rows_o, RANK), h, 0, 512)
-        old_o = decoded(wo[:, :, :, at_o].reshape(rows_o, 512))
-        copy_o[:, at_o] = (old_o - learn_rate * all_o).astype(jnp.bfloat16)
-        all_q = step(pf[:, :, :32, :].reshape(rows_q, RANK), h, 512, 256)
-        old_q = decoded(wq[:, :, :, at_q].reshape(rows_q, 256))
-        copy_q[:, at_q] = (old_q - learn_rate * all_q).astype(jnp.bfloat16)
-
-    @pl.when(own)
-    def _():
-        for h in range(2):
-            at_o, at_q = pl.ds(512 * h, 512), pl.ds(256 * h, 256)
-            mine_o = step(proj_o[...], h, 0, 512)
-            step_o[:, at_o] = mine_o
-            new_o[:, at_o] = weight_o[:, at_o] - learn_rate * mine_o
-            mine_q = step(proj_q[...], h, 512, 256)
-            step_q[:, at_q] = mine_q
-            new_q[:, at_q] = weight_q[:, at_q] - learn_rate * mine_q
-            nf_o[:, at_o], ns_o[:, at_o], _ = moment_update(
-                low[h, :, :512], first_o[:, at_o], second_o[:, at_o]
-            )
-            nf_q[:, at_q], ns_q[:, at_q], _ = moment_update(
-                low[h, :, 512:], first_q[:, at_q], second_q[:, at_q]
-            )
-
-
-STEPS = 4
+        mine_o = scale * product(proj_o[...], h, 0, 512)
+        step_o[:, at_o] = mine_o
+        new_o[:, at_o] = weight_o[:, at_o] - learn_rate * mine_o
+        mine_q = scale * product(proj_q[...], h, 512, 256)
+        step_q[:, at_q] = mine_q
+        new_q[:, at_q] = weight_q[:, at_q] - learn_rate * mine_q
+        nf_o[:, at_o], ns_o[:, at_o], _ = moment_update(
+            low[h, :, :512], first_o[:, at_o], second_o[:, at_o]
+        )
+        nf_q[:, at_q], ns_q[:, at_q], _ = moment_update(
+            low[h, :, 512:], first_q[:, at_q], second_q[:, at_q]
+        )
+    new_copies = [
+        pltpu.make_async_copy(src, dst, new_sems.at[k])
+        for k, (src, dst) in enumerate(zip(new, (
+            new_q_out, new_o_out, step_q_out, step_o_out, nf_q_out, ns_q_out, nf_o_out, ns_o_out
+        )))
+    ]
+    for c in new_copies:
+        c.start()
+    for i in range(CHUNKS):
+        for c in out_copies(i):
+            c.wait()
+    for c in new_copies:
+        c.wait()
 
 
 def finished(pf, wq, wo, half, low, total, proj_q, proj_o, weight_q, weight_o,
              first_q, second_q, first_o, second_o):
     f32, bf16 = jnp.float32, jnp.bfloat16
-
-    def blocks(shape):
-        rest = (0,) * (len(shape) - 1)
-        return pl.BlockSpec((shape[0] // STEPS,) + tuple(shape[1:]), lambda i: (i,) + rest)
-
-    def whole(shape):
-        return pl.BlockSpec(tuple(shape), lambda i: (0,) * len(shape))
-
-    small = (half, low, total, proj_q, proj_o, weight_q, weight_o, first_q, second_q, first_o, second_o)
+    anywhere = pl.BlockSpec(memory_space=pl.ANY)
+    dma = pltpu.SemaphoreType.DMA
+    small = (low, total, proj_q, proj_o, weight_q, weight_o, first_q, second_q, first_o, second_o)
     outs = (
         ((64, 512), f32), ((32, 1024), f32), ((64, 512), f32), ((32, 1024), f32),
         ((8, 512), f32), ((8, 512), f32), ((8, 1024), f32), ((8, 1024), f32),
@@ -485,12 +543,19 @@
     )
     return pl.pallas_call(
         final_kernel,
-        grid=(STEPS,),
         out_shape=tuple(jax.ShapeDtypeStruct(*s) for s in outs),
-        in_specs=[blocks(a.shape) for a in (pf, wq, wo)] + [whole(a.shape) for a in small],
-        out_specs=tuple(whole(s) for s, _ in outs[:8]) + tuple(blocks(s) for s, _ in outs[8:]),
+        in_specs=[anywhere] * 14,
+        out_specs=(anywhere,) * 10,
+        scratch_shapes=[
+            *(pltpu.VMEM(a.shape, a.dtype) for a in (pf, wq, wo, half)),
+            pltpu.VMEM((RANK, 2 * HALF), bf16),
+            tuple(pltpu.VMEM(a.shape, a.dtype) for a in small),
+            tuple(pltpu.VMEM(*s) for s in outs[:8]),
+            *(pltpu.VMEM(*s) for s in outs[8:]),
+            dma((3, CHUNKS)), dma((len(small) + 1,)), dma((8,)), dma((2, CHUNKS)),
+        ],
         cost_estimate=pl.CostEstimate(flops=2_200_000_000, bytes_accessed=12_000_000, transcendentals=0),
-    )(pf, wq, wo, *small)
+    )(pf, wq, wo, half, *small)
 
 
 def local(

time: 66 us -> 63.7 us (0.965)
  Pallas kernels: 65.2 us -> 62.6 us
    pallas_call x1, Pallas kernels: 7.97 us -> 6.15 us  [finished(): pl.pallas_call(final_kernel, out_shape=tuple((jax.ShapeDtypeStruct(*s) fo...]
    pallas_call x1, Pallas kernels: 57.2 us -> 56.5 us  [gathered(): pl.pallas_call(comm_kernel, out_shape=tuple((jax.ShapeDtypeStruct(*s) for...]
where the time goes in v6:
time: 63.7 us; the launch traced here: 63.3 us
  Pallas kernels  62.6 us (98%)
  between operations  0.65 us (1%)
    pallas_call x1, Pallas kernels, gathered(): pl.pallas_call(comm_kernel, out_shape=tuple((jax.ShapeDtypeStruct(*s) for...  56.5 us
    pallas_call x1, Pallas kernels, finished(): pl.pallas_call(final_kernel, out_shape=tuple((jax.ShapeDtypeStruct(*s) fo...  6.15 us

profile of v6, /device:TPU:1, one launch (start us, length us, event | category | flops | bytes accessed | tf_op | source)
XLA Modules:
  0.0 63.3 jit_solution(6795442321400099824)
XLA Ops:
  0.6 56.5 %shard_map.195 = (bf16[32,2,48,256]{3,2,1,0:T(8,128)(2,1)}, bf16[2,32,8,768]{3,2,1,0:T(8,128)(2,1)}, f32[2,8,768]{2,1,0:T(8,128)}, f32[1,128]{1,0:T(1,128)}, bf1...) custom-call(bf16[128,2048]{1,0:T(8,128)(2,1)} %inputs.1, bf16[128,512]{1,0:T(8,128)(2,1)} %query_cot.1, ...), custom_call_target="tpu_custom_call" | custom-call | tf_op jit(solution)/shard_map/pallas_call | solution.py:376
  57.1 6.2 %shard_map.196 = (f32[64,512]{1,0:T(8,128)}, f32[32,1024]{1,0:T(8,128)}, f32[64,512]{1,0:T(8,128)}, f32[32,1024]{1,0:T(8,128)}, f32[8,512]{1,0:T(8,128)}, /*inde...) custom-call(bf16[32,2,48,256]{3,2,1,0:T(8,128)(2,1)} %get-tuple-elem, ...), custom_call_target="tpu_custom_call" | custom-call | flops 2200000000 | bytes 12000000 | tf_op jit(solution)/shard_map/pallas_call | solution.py:544

commit v7 on v6

--- a/solution.py
+++ b/solution.py
@@ -48,7 +48,7 @@
     pf_out, half_out, low_out, total_out, wg_q, wg_o,
     pf, half, low,
     x_in, c_q, x_at, c_o, fst, snd, old_q, old_o, code_q, code_o,
-    lb_o, lb_q, cb_o, cb_q, by_o, by_q, bx_o, bx_q, sz, bz, ty, by2, qz, qx, qy, qt,
+    lb_o, lb_q, cb_o, cb_q, by_o, by_q, bx_o, bx_q, sz, bz, ty, by2, qz, qx, qy,
     loc, sent, a_z, a_x, a_c, w_x, w_z, w_d, w_y, b_y, b_x, b_z, b_2, b_l,
     e_z, e_x, e_y, q_z, q_x, q_y,
 ):
@@ -293,35 +293,40 @@
     arrived(by2, b_2.at[0])
 
     low_sum = mine + by2[...]
-    low[p] = low_sum
+    low[...] = low_sum
     _, _, normed = moment_update(low_sum, fst[p], snd[p])
-    half[p, f] = normed.astype(jnp.bfloat16)
+    half[f] = normed.astype(jnp.bfloat16)
     square = normed * normed
     total = square[:, 0:128]
     for k in range(1, 6):
         total = total + square[:, k * 128 : (k + 1) * 128]
     qz[z * 2 + t] = jnp.sum(total, axis=0, keepdims=True)
 
-    def piece(g, n, par):
-        return half.at[par, pl.ds(g, n)]
+    def piece(g, n):
+        return half.at[pl.ds(g, n)]
+
+    def half_piece(g):
+        return half_out.at[p, pl.ds(g, 2)]
 
     for d in NEAR_FIRST:
-        send(piece(f, 1, p), piece(f, 1, p), 11, e_z.at[d], at_z(d))
+        send(piece(f, 1), piece(f, 1), 11, e_z.at[d], at_z(d))
     for d in range(NZ):
         for core, dev in ((0, at_z(d)), (1, at_zt(d) if d else other_core)):
             if d or core:
                 row = qz.at[z * 2 + t]
                 send(row, row, 13, q_z.at[0], dev)
-    send(low.at[p], low.at[p], 10, b_l.at[0], at_y(1))
+    send(low, low_out.at[p], 10, b_l.at[0], at_y(1))
+    outs.append(pltpu.make_async_copy(low, low_out.at[p], loc.at[3]))
+    outs[-1].start()
     query_y(4)
     output_y(5)
     output_y(4)
     for d in (0,) + NEAR_FIRST:
         g = ((z + NZ - d) % NZ) * NX + x
         if d:
-            arrived(piece(g, 1, p), e_z.at[d])
+            arrived(piece(g, 1), e_z.at[d])
         for e in (2, 1, 3):
-            send(piece(g, 1, p), piece(g, 1, p), 11, e_x.at[d], at_x(e))
+            send(piece(g, 1), piece(g, 1), 11, e_x.at[d], at_x(e))
     arrived(qz.at[pl.ds(0, 2 * NZ - 1)], q_z.at[0])
     total = qz[0]
     for k in range(1, 2 * NZ):
@@ -331,24 +336,20 @@
         send(qx.at[x], qx.at[x], 14, q_x.at[0], at_x(e))
     for d in (0,) + NEAR_FIRST:
         row = rows_at(d)
-        arrived(piece(0, 3, p), e_x.at[d])
+        arrived(piece(0, 3), e_x.at[d])
         for side in range(2):
-            two = piece(row + 2 * side, 2, p)
-            send(two, two, 12, e_y.at[0], at_y(1 if side == 0 else NY - 1))
+            two = piece(row + 2 * side, 2)
+            send(two, half_piece(row + 2 * side), 12, e_y.at[0], at_y(1 if side == 0 else NY - 1))
+    outs.append(pltpu.make_async_copy(half, half_out.at[p], loc.at[2]))
+    outs[-1].start()
     arrived(qx.at[pl.ds(0, 3)], q_x.at[0])
-    qy[p] = (qx[0] + qx[1]) + (qx[2] + qx[3])
-    send(qy.at[p], qy.at[p], 15, q_y.at[0], at_y(1))
-    arrived(low.at[o], b_l.at[0])
-    arrived(piece(0, 32, o), e_y.at[0])
-    arrived(qy.at[o], q_y.at[0])
-    qt[...] = qy[0] + qy[1]
-    outs += [
-        pltpu.make_async_copy(half, half_out, loc.at[2]),
-        pltpu.make_async_copy(low, low_out, loc.at[3]),
-        pltpu.make_async_copy(qt, total_out, loc.at[4]),
-    ]
-    for c in outs[1:]:
-        c.start()
+    qy[...] = (qx[0] + qx[1]) + (qx[2] + qx[3])
+    send(qy, total_out.at[p], 15, q_y.at[0], at_y(1))
+    outs.append(pltpu.make_async_copy(qy, total_out.at[p], loc.at[4]))
+    outs[-1].start()
+    arrived(low_out.at[o], b_l.at[0])
+    arrived(half_out.at[o], e_y.at[0])
+    arrived(total_out.at[o], q_y.at[0])
     arrived(wg_q.at[:, o], w_y.at[0])
     arrived(wg_o.at[:, o], w_y.at[1])
     for c in outs:
@@ -356,8 +357,8 @@
     for kind, ref in enumerate((
         pf.at[pl.ds(0, 31), 0], pf.at[:, 0],
         wg_q.at[pl.ds(0, 31), 0], wg_q.at[:, 0], wg_o.at[pl.ds(0, 31), 0], wg_o.at[:, 0],
-        by_o, by_q, bz, by2, low.at[0], piece(0, 31, 0), piece(0, 32, 0),
-        qz.at[pl.ds(0, 2 * NZ - 1)], qx.at[pl.ds(0, 3)], qy.at[0],
+        by_o, by_q, bz, by2, low, piece(0, 31), piece(0, 32),
+        qz.at[pl.ds(0, 2 * NZ - 1)], qx.at[pl.ds(0, 3)], qy,
         bx_o, bx_q,
     )):
         remote(ref, ref, sent.at[kind], sent.at[kind], other_core).wait_send()
@@ -368,21 +369,18 @@
     f32, bf16 = jnp.float32, jnp.bfloat16
     anywhere = pl.BlockSpec(memory_space=pl.ANY)
     dma = pltpu.SemaphoreType.DMA
-    shared = (
-        ((32, 2, 48, RANK), bf16),
-        ((2, 32, 8, HALF), bf16),
-        ((2, 8, HALF), f32),
-    )
+    own_sides = (((32, 2, 48, RANK), bf16), ((32, 8, HALF), bf16), ((8, HALF), f32))
+    both_sides = own_sides[:1] + tuple(((2,) + shape, kind) for shape, kind in own_sides[1:])
     return pl.pallas_call(
         comm_kernel,
-        out_shape=tuple(jax.ShapeDtypeStruct(*s) for s in shared) + (
-            jax.ShapeDtypeStruct((1, 128), f32),
+        out_shape=tuple(jax.ShapeDtypeStruct(*s) for s in both_sides) + (
+            jax.ShapeDtypeStruct((2, 1, 128), f32),
             jax.ShapeDtypeStruct((32, 2, 32, 512), bf16),
             jax.ShapeDtypeStruct((32, 2, 16, 1024), bf16),
         ),
         in_specs=[anywhere] * 12,
         out_specs=(anywhere,) * 6,
-        scratch_shapes=[pltpu.VMEM(*s) for s in shared] + [
+        scratch_shapes=[pltpu.VMEM(*s) for s in own_sides] + [
             pltpu.VMEM((128, D), bf16),
             pltpu.VMEM((128, 512), bf16),
             pltpu.VMEM((128, DA), bf16),
@@ -407,7 +405,6 @@
             pltpu.VMEM((8, HALF), f32),
             pltpu.VMEM((2 * NZ, 1, 128), f32),
             pltpu.VMEM((NX, 1, 128), f32),
-            pltpu.VMEM((2, 1, 128), f32),
             pltpu.VMEM((1, 128), f32),
             dma((16,)), dma((18,)), dma((2, 8)), dma((2, 8)), dma((2,)), dma((9,)), dma((5, 2)), dma((8,)), dma((2,)),
             dma((2, 6)), dma((2,)), dma((1,)), dma((1,)), dma((1,)),
@@ -462,7 +459,7 @@
 
     half_load.wait()
     small_loads[1].wait()
-    mean = jnp.sum(total[...], axis=1, keepdims=True) / (RANK * (DA + D))
+    mean = jnp.sum(total[0] + total[1], axis=1, keepdims=True) / (RANK * (DA + D))
     scale = lax.rsqrt(mean + mean_eps)
     rate = learn_rate * scale
     for h in range(2):

time: 63.7 us -> 62.8 us (0.986)
  Pallas kernels: 62.6 us -> 61.8 us
    pallas_call x1, Pallas kernels: 56.5 us -> 55.7 us  [gathered(): pl.pallas_call(comm_kernel, out_shape=tuple((jax.ShapeDtypeStruct(*s) for...]
where the time goes in v7:
time: 62.8 us; the launch traced here: 62.5 us
  Pallas kernels  61.8 us (98%)
  between operations  0.65 us (1%)
    pallas_call x1, Pallas kernels, gathered(): pl.pallas_call(comm_kernel, out_shape=tuple((jax.ShapeDtypeStruct(*s) for...  55.7 us
    pallas_call x1, Pallas kernels, finished(): pl.pallas_call(final_kernel, out_shape=tuple((jax.ShapeDtypeStruct(*s) fo...  6.16 us

profile of v7, /device:TPU:1, one launch (start us, length us, event | category | flops | bytes accessed | tf_op | source)
XLA Modules:
  0.0 62.5 jit_solution(13141619340899302741)
XLA Ops:
  0.6 55.7 %shard_map.195 = (bf16[32,2,48,256]{3,2,1,0:T(8,128)(2,1)}, bf16[2,32,8,768]{3,2,1,0:T(8,128)(2,1)}, f32[2,8,768]{2,1,0:T(8,128)}, f32[2,1,128]{2,1,0:T(1,128)},...) custom-call(bf16[128,2048]{1,0:T(8,128)(2,1)} %inputs.1, bf16[128,512]{1,0:T(8,128)(2,1)} %query_cot.1, ...), custom_call_target="tpu_custom_call" | custom-call | tf_op jit(solution)/shard_map/pallas_call | solution.py:374
  56.3 6.2 %shard_map.196 = (f32[64,512]{1,0:T(8,128)}, f32[32,1024]{1,0:T(8,128)}, f32[64,512]{1,0:T(8,128)}, f32[32,1024]{1,0:T(8,128)}, f32[8,512]{1,0:T(8,128)}, /*inde...) custom-call(bf16[32,2,48,256]{3,2,1,0:T(8,128)(2,1)} %get-tuple-elem, ...), custom_call_target="tpu_custom_call" | custom-call | flops 2200000000 | bytes 12000000 | tf_op jit(solution)/shard_map/pallas_call | solution.py:541

commit v8 on v7

--- a/solution.py
+++ b/solution.py
@@ -278,6 +278,7 @@
         send(sz.at[(z + d) % NZ], bz.at[d - 1], 8, b_z.at[0], at_z(d))
     output_y(2)
     query_z(3)
+    output_y(6)
     arrived(bz, b_z.at[0])
     mine = jnp.concatenate([lb_o[o, 0, z], lb_q[o, 0, z]], axis=1)
     for d in range(7):
@@ -285,7 +286,6 @@
     ty[...] = mine
     send(ty, by2, 9, b_2.at[0], at_y(2))
     query_y(3)
-    output_y(6)
     output_y(3)
     query_z(4)
     for c in loads[8:16]:
@@ -308,7 +308,7 @@
     def half_piece(g):
         return half_out.at[p, pl.ds(g, 2)]
 
-    for d in NEAR_FIRST:
+    for d in (4, 3, 5, 2, 6, 1, 7):
         send(piece(f, 1), piece(f, 1), 11, e_z.at[d], at_z(d))
     for d in range(NZ):
         for core, dev in ((0, at_z(d)), (1, at_zt(d) if d else other_core)):

time: 62.8 us -> 62 us (0.987)
  Pallas kernels: 61.8 us -> 60.8 us
    pallas_call x1, Pallas kernels: 55.7 us -> 54.6 us  [gathered(): pl.pallas_call(comm_kernel, out_shape=tuple((jax.ShapeDtypeStruct(*s) for...]
where the time goes in v8:
time: 62 us; the launch traced here: 61.5 us
  Pallas kernels  60.8 us (98%)
  between operations  0.65 us (1%)
    pallas_call x1, Pallas kernels, gathered(): pl.pallas_call(comm_kernel, out_shape=tuple((jax.ShapeDtypeStruct(*s) for...  54.6 us
    pallas_call x1, Pallas kernels, finished(): pl.pallas_call(final_kernel, out_shape=tuple((jax.ShapeDtypeStruct(*s) fo...  6.16 us

profile of v8, /device:TPU:1, one launch (start us, length us, event | category | flops | bytes accessed | tf_op | source)
XLA Modules:
  0.0 61.5 jit_solution(13936081006252199420)
XLA Ops:
  0.6 54.6 %shard_map.195 = (bf16[32,2,48,256]{3,2,1,0:T(8,128)(2,1)}, bf16[2,32,8,768]{3,2,1,0:T(8,128)(2,1)}, f32[2,8,768]{2,1,0:T(8,128)}, f32[2,1,128]{2,1,0:T(1,128)},...) custom-call(bf16[128,2048]{1,0:T(8,128)(2,1)} %inputs.1, bf16[128,512]{1,0:T(8,128)(2,1)} %query_cot.1, ...), custom_call_target="tpu_custom_call" | custom-call | tf_op jit(solution)/shard_map/pallas_call | solution.py:374
  55.3 6.2 %shard_map.196 = (f32[64,512]{1,0:T(8,128)}, f32[32,1024]{1,0:T(8,128)}, f32[64,512]{1,0:T(8,128)}, f32[32,1024]{1,0:T(8,128)}, f32[8,512]{1,0:T(8,128)}, /*inde...) custom-call(bf16[32,2,48,256]{3,2,1,0:T(8,128)(2,1)} %get-tuple-elem, ...), custom_call_target="tpu_custom_call" | custom-call | flops 2200000000 | bytes 12000000 | tf_op jit(solution)/shard_map/pallas_call | solution.py:541
